TPU v7x, 32 devices: a whole 2x2x4 slice. The times are simulated.
32 devices in a mesh: ep: 16 (over z, y, x), tp: 2 (over core).
Axes of the slice: x: 2, y: 2, z: 4, core: 2. Of those that a mesh axis runs over, the one named last changes fastest.
Arguments:
- hidden: bfloat16 [1024, 2048], P('ep'), may hold values from -6 to 6
- mix_gain: float32 [2048], replicated, may hold values from 0.1 to 1.9
- recept_weight: bfloat16 [2048, 1024], P(None, 'tp'), may hold values from -0.125 to 0.125
- key_weight: bfloat16 [2048, 1024], P(None, 'tp'), may hold values from -0.125 to 0.125
- value_weight: bfloat16 [2048, 1024], P(None, 'tp'), may hold values from -0.125 to 0.125
- decay_down: bfloat16 [2048, 64], replicated, may hold values from -0.125 to 0.125
- decay_up: bfloat16 [64, 1024], replicated, may hold values from -0.75 to 0.75
- decay_bias: float32 [1024], replicated, may hold values from -4 to 1
- rate_down: bfloat16 [2048, 64], replicated, may hold values from -0.125 to 0.125
- rate_up: bfloat16 [64, 1024], replicated, may hold values from -0.75 to 0.75
- rate_bias: float32 [1024], replicated, may hold values from -4 to 4
- head_gain: float32 [1024], replicated, may hold values from 0.1 to 1.9
- out_weight: bfloat16 [1024, 2048], P('tp'), may hold values from -0.1875 to 0.1875
- memory_state: float32 [1024, 16, 64, 64], P('ep', 'tp'), may hold values from -6 to 6
- ffn_gain: float32 [2048], replicated, may hold values from 0.1 to 1.9
- blend_vector: bfloat16 [2048], replicated, may hold values from -0.125 to 0.125
- dense_gate: bfloat16 [2048, 5632], P(None, ('ep', 'tp')), may hold values from -0.125 to 0.125
- dense_up: bfloat16 [2048, 5632], P(None, ('ep', 'tp')), may hold values from -0.125 to 0.125
- dense_down: bfloat16 [5632, 2048], P(('ep', 'tp')), may hold values from -0.3125 to 0.3125
- expert_gate: bfloat16 [16, 2048, 1536], P('ep', None, 'tp'), may hold values from -0.125 to 0.125
- expert_up: bfloat16 [16, 2048, 1536], P('ep', None, 'tp'), may hold values from -0.125 to 0.125
- expert_down: bfloat16 [16, 1536, 2048], P('ep', 'tp'), may hold values from -0.15625 to 0.15625
- routing: int32 [1024, 2], P('ep'), may hold values from 0 to 15, all different within a row; in each aligned block of 64 rows (0 to 63, 64 to 127, ...) at most 16 rows name the same one
- route_scale: float32 [1024, 2], P('ep'), may hold values from 0.25 to 1
Outputs:
- layer_out: bfloat16 [1024, 2048], P('ep')
- new_state: float32 [1024, 16, 64, 64], P('ep', 'tp')
Inputs may be any that keep to these rules, and one draw needn't show every extreme that they name: `routing`: among the 64 sequences of one index of ep, no expert is chosen more than 16 times, and some expert is chosen exactly 16 times; a sequence's 2 choices differ.
All inputs are finite; a program needn't handle non-finite values.
Results may differ from a plain program's by a relative error of at most 0.017.
Values may be sent and summed in bfloat16 or wider, within the bound.
No kernel may reach another device: no remote copies, remote signals or barrier semaphores. Data moves between devices by JAX's collectives and lax.ppermute only.
A program may use at most 192 MiB of HBM per device.

v0:
```python
import functools
import math

import jax
import jax.numpy as jnp
from jax import lax
from jax.experimental import pallas as pl
from jax.experimental.pallas import tpu as pltpu
from jax.sharding import PartitionSpec as P


def rms_scaled(tensor, gain_vec):
    values = tensor.astype(jnp.float32)
    return values * lax.rsqrt(jnp.mean(values * values, axis=-1, keepdims=True) + 1e-06) * gain_vec


def silu_of(tensor):
    return tensor / (1.0 + jnp.exp(-tensor))


def matmul(left, right):
    return jnp.dot(left, right, preferred_element_type=jnp.float32)


def touch_kernel(*refs):
    refs[-1][0] = refs[0][0]


def touch(chip, *values):
    smem = pl.BlockSpec(memory_space=pltpu.SMEM)
    return pl.pallas_call(
        touch_kernel,
        in_specs=[smem] + [pl.BlockSpec(memory_space=pltpu.VMEM)] * len(values),
        out_specs=smem,
        out_shape=jax.ShapeDtypeStruct(chip.shape, chip.dtype),
        compiler_params=pltpu.CompilerParams(vmem_limit_bytes=12 * 1024 * 1024),
        name="touch",
    )(chip, *values)


def experts_kernel(
    pieces,
    cap,
    span,
    chip_ref,
    expert_gate_ref,
    expert_up_ref,
    expert_down_ref,
    dense_gate_ref,
    dense_up_ref,
    dense_down_ref,
    blend_ref,
    *refs,
):
    ins, outs = refs[: len(pieces)], refs[len(pieces) : 2 * len(pieces)]
    token_scr, act_scr = refs[2 * len(pieces) :]
    width = dense_down_ref.shape[-1]
    count, _ = ins[0].shape
    slots = len(pieces) // 2 * (count // span) * cap
    named = chip_ref[0].astype(jnp.float32)
    turn = lambda left, right: lax.dot_general(
        left, right, (((1,), (1,)), ((), ())), preferred_element_type=jnp.float32
    )
    row = lax.broadcasted_iota(jnp.int32, (count, 1), 0)
    lane = lax.broadcasted_iota(jnp.int32, (count, slots), 1)
    selects, weights = [], []
    for piece, ((scale_first, scale_rest, offset, inner), ref) in enumerate(zip(pieces, ins)):
        marks = ref[:, width:].astype(jnp.float32)
        block = row // span
        base = (block // inner) * scale_first + block % inner * scale_rest + offset
        slot = jnp.full((count, 1), -1, jnp.int32)
        weight = jnp.zeros((count, 1), jnp.float32)
        for choice in range(2):
            mark = lambda k: marks[:, 4 * choice + k : 4 * choice + k + 1]
            hit = mark(0) == named
            slot = jnp.where(hit, base * cap + mark(1).astype(jnp.int32), slot)
            weight = jnp.where(hit, mark(2) + mark(3), weight)
        selects.append(jnp.where(lane == slot, 1.0, 0.0).astype(jnp.bfloat16))
        weights.append(weight)
        token_scr[piece * count : (piece + 1) * count, :] = ref[:, :width]
    select = jnp.concatenate(selects)
    picked = lax.dot_general(
        select, token_scr[...], (((0,), (0,)), ((), ())), preferred_element_type=jnp.float32
    ).astype(jnp.bfloat16)
    tokens = token_scr[...]
    blend_rows = jnp.broadcast_to(blend_ref[...], (8, width))
    blend = 1.0 / (1.0 + jnp.exp(-turn(tokens, blend_rows)[:, :1]))
    act_scr[...] = (
        silu_of(turn(tokens, dense_gate_ref[...])) * turn(tokens, dense_up_ref[...]) * blend
    ).astype(jnp.bfloat16)
    gate = silu_of(matmul(picked, expert_gate_ref[0]))
    expert_act = (gate * matmul(picked, expert_up_ref[0])).astype(jnp.bfloat16)
    expert_out = matmul(expert_act, expert_down_ref[0]).astype(jnp.bfloat16)
    for piece in range(len(pieces)):
        outs[piece][...] = (
            matmul(selects[piece], expert_out) * weights[piece]
            + matmul(act_scr[piece * count : (piece + 1) * count, :], dense_down_ref[...])
        ).astype(jnp.bfloat16)


def experts(own, other, cap, span, chip, weights):
    sides, (firsts, group, _, wide) = len(own), own[0].shape
    count = firsts * group * span
    flat = [value.reshape(count, wide) for value in own + other]
    pieces = [(group, 1, s * firsts * group, group) for s in range(sides)]
    pieces += [(firsts * group, 1, s * group, group) for s in range(sides)]
    width = weights[2].shape[-1]
    vmem = pl.BlockSpec(memory_space=pltpu.VMEM)
    units = weights[0].shape[-1]
    rows = 2 * sides * count
    outs = pl.pallas_call(
        functools.partial(experts_kernel, tuple(pieces), cap, span),
        in_specs=[pl.BlockSpec(memory_space=pltpu.SMEM)] + [vmem] * (len(weights) + len(flat)),
        out_specs=[vmem] * len(flat),
        out_shape=[jax.ShapeDtypeStruct((count, width), jnp.bfloat16)] * len(flat),
        scratch_shapes=[
            pltpu.VMEM((rows, width), jnp.bfloat16),
            pltpu.VMEM((rows, weights[3].shape[0]), jnp.bfloat16),
        ],
        compiler_params=pltpu.CompilerParams(vmem_limit_bytes=16 * 1024 * 1024 + rows * 24000),
        cost_estimate=pl.CostEstimate(
            flops=6 * rows * width * 2 * units, bytes_accessed=6 * width * units, transcendentals=0
        ),
        name="experts",
    )(chip, *weights, *flat)
    outs = [value.reshape(firsts, group, span, width) for value in outs]
    return outs[:sides], outs[sides:]


def grid_of(count):
    side = max(1, int(round((count / 4) ** 0.5)))
    if 4 * side * side == count:
        return (4, side, side)
    return (count, 1, 1)


def turned(index, dims, axis, step):
    place = [index // (dims[1] * dims[2]), index // dims[2] % dims[1], index % dims[2]]
    place[axis] = (place[axis] + step) % dims[axis]
    return (place[0] * dims[1] + place[1]) * dims[2] + place[2]


def hop(value, dims, axes, step):
    count = dims[0] * dims[1] * dims[2]
    perm = [
        (2 * chip + core, 2 * turned(chip, dims, axes[core], step) + core)
        for chip in range(count)
        for core in range(2)
    ]
    return lax.ppermute(value, ("ep", "tp"), perm)


def swap(value):
    return lax.ppermute(value, "tp", [(0, 1), (1, 0)])


LINE, FIRST, SECOND = (0, 0), (2, 1), (1, 2)


def total(*values):
    return sum(value.astype(jnp.float32) for value in values).astype(jnp.bfloat16)


def plane_gather(blocks, dims):
    near = range(1, dims[1])
    firsts = jnp.stack([blocks] + [hop(blocks, dims, FIRST, k) for k in near])
    own = [firsts] + [hop(firsts, dims, SECOND, k) for k in near]
    other = [swap(own[0])]
    return own, other + [swap(value) for value in own[1:]]


def plane_reduce(own, other, dims):
    near = range(1, dims[1])
    back = [swap(other[k]) for k in near]
    back = [swap(other[0])] + back
    arrived = [hop(total(own[k], back[k]), dims, SECOND, -k) for k in near]
    firsts = total(own[0], back[0], *arrived)
    return total(firsts[0], *[hop(firsts[k], dims, FIRST, -k) for k in near])


def attention_kernel(
    core_ref,
    hidden_ref,
    mix_ref,
    recept_ref,
    key_ref,
    value_ref,
    decay_down_ref,
    decay_up_ref,
    decay_bias_ref,
    rate_down_ref,
    rate_up_ref,
    rate_bias_ref,
    gain_ref,
    out_weight_ref,
    state_ref,
    kept_ref,
    sent_ref,
    new_ref,
    unit_scr,
    pull_scr,
    push_scr,
    decay_scr,
    recept_scr,
    value_scr,
    head_scr,
):
    heads, seqs, size = unit_scr.shape
    block = state_ref.shape[0]
    step = pl.program_id(0)

    def flat_dot(left, right):
        return lax.dot_general(
            left, right, (((1,), (1,)), ((), ())), preferred_element_type=jnp.float32
        )

    @pl.when(step == 0)
    def _():
        normed = rms_scaled(hidden_ref[...], mix_ref[...]).astype(jnp.bfloat16)
        rounded = lambda value: value.astype(jnp.bfloat16).astype(jnp.float32)
        recept = rounded(matmul(normed, recept_ref[...]))
        key = rounded(matmul(normed, key_ref[...]))
        value = rounded(matmul(normed, value_ref[...]))
        decay_low = jnp.tanh(flat_dot(normed, decay_down_ref[...])).astype(jnp.bfloat16)
        decay_pre = matmul(decay_low, decay_up_ref[...]) + decay_bias_ref[...]
        decay = jnp.exp(-math.exp(-0.5) / (1.0 + jnp.exp(-decay_pre)))
        rate_low = flat_dot(normed, rate_down_ref[...]).astype(jnp.bfloat16)
        rate = 1.0 / (1.0 + jnp.exp(-(matmul(rate_low, rate_up_ref[...]) + rate_bias_ref[...])))
        for head in range(heads):
            cut = slice(head * size, (head + 1) * size)
            own_key = key[:, cut]
            unit = own_key * lax.rsqrt(
                jnp.sum(own_key * own_key, axis=-1, keepdims=True) + 1e-06
            )
            unit_scr[head] = unit
            pull_scr[head] = unit * rate[:, cut]
            push_scr[head] = own_key * rate[:, cut]
            decay_scr[head] = decay[:, cut]
            recept_scr[head] = recept[:, cut]
            value_scr[head] = value[:, cut]

    rows = pl.ds(pl.multiple_of(step * block, block), block)
    ones = jnp.ones((size, 128), jnp.bfloat16)
    lane = lax.broadcasted_iota(jnp.int32, (size, 128), 1)
    for head in range(heads):
        unit = unit_scr[head, rows, :]
        products = [
            (state_ref[seq, head] * unit[seq : seq + 1]).astype(jnp.bfloat16)
            for seq in range(block)
        ]
        removed = matmul(jnp.concatenate(products), ones)
        pull = pull_scr[head, rows, :]
        push = push_scr[head, rows, :]
        decay = decay_scr[head, rows, :]
        recept = recept_scr[head, rows, :]
        value = value_scr[head, rows, :].T
        products = []
        for seq in range(block):
            one = slice(seq, seq + 1)
            fresh = (
                state_ref[seq, head] * decay[one]
                - removed[seq * size : (seq + 1) * size, :size] * pull[one]
                + value[:, one] * push[one]
            )
            new_ref[seq, head] = fresh
            products.append((fresh * recept[one]).astype(jnp.bfloat16))
        readout = matmul(jnp.concatenate(products), ones)
        columns = jnp.zeros((size, 128), jnp.float32)
        for seq in range(block):
            columns = jnp.where(lane == seq, readout[seq * size : (seq + 1) * size], columns)
        lines = columns.T[:block]
        centred = lines - jnp.mean(lines, axis=-1, keepdims=True)
        variance = jnp.mean(centred * centred, axis=-1, keepdims=True)
        head_scr[head, rows, :] = (
            centred
            * lax.rsqrt(variance + 0.00064)
            * gain_ref[:, head * size : (head + 1) * size]
        )

    @pl.when(step == pl.num_programs(0) - 1)
    def _():
        half = seqs // 2
        for side, ref in ((core_ref[0], kept_ref), (1 - core_ref[0], sent_ref)):
            picked = pl.ds(pl.multiple_of(side * half, half), half)
            lines = jnp.concatenate([head_scr[head, picked, :] for head in range(heads)], axis=1)
            ref[...] = matmul(lines.astype(jnp.bfloat16), out_weight_ref[...]).astype(ref.dtype)


def attention(
    hidden,
    mix_gain,
    recept_weight,
    key_weight,
    value_weight,
    decay_down,
    decay_up,
    decay_bias,
    rate_down,
    rate_up,
    rate_bias,
    head_gain,
    out_weight,
    memory_state,
):
    seqs, width = hidden.shape
    _, heads, size, _ = memory_state.shape
    own = heads * size
    low = decay_down.shape[1]
    block = 8
    core = lax.axis_index("tp").astype(jnp.int32).reshape(1)
    whole = lambda *shape: pl.BlockSpec(shape, lambda i, c: (0,) * len(shape))
    half = lambda rows: pl.BlockSpec((rows, own), lambda i, c: (0, c[0]))
    state_spec = pl.BlockSpec((block, heads, size, size), lambda i, c: (i, 0, 0, 0))
    per_head = pltpu.VMEM((heads, seqs, size), jnp.float32)
    return pl.pallas_call(
        attention_kernel,
        grid_spec=pltpu.PrefetchScalarGridSpec(
            num_scalar_prefetch=1,
            grid=(seqs // block,),
            in_specs=[
                whole(seqs, width),
                whole(1, width),
                whole(width, own),
                whole(width, own),
                whole(width, own),
                whole(low, width),
                half(low),
                half(1),
                whole(low, width),
                half(low),
                half(1),
                half(1),
                whole(own, width),
                state_spec,
            ],
            out_specs=[whole(seqs // 2, width), whole(seqs // 2, width), state_spec],
            scratch_shapes=[per_head] * 7,
        ),
        out_shape=[
            jax.ShapeDtypeStruct((seqs // 2, width), jnp.bfloat16),
            jax.ShapeDtypeStruct((seqs // 2, width), jnp.bfloat16),
            jax.ShapeDtypeStruct(memory_state.shape, memory_state.dtype),
        ],
        compiler_params=pltpu.CompilerParams(
            dimension_semantics=("arbitrary",), vmem_limit_bytes=66000000
        ),
        name="attention",
    )(
        core,
        hidden,
        mix_gain[None],
        recept_weight,
        key_weight,
        value_weight,
        decay_down.T,
        decay_up,
        decay_bias[None],
        rate_down.T,
        rate_up,
        rate_bias[None],
        head_gain[None],
        out_weight,
        memory_state,
    )


def shards(
    hidden,
    mix_gain,
    recept_weight,
    key_weight,
    value_weight,
    decay_down,
    decay_up,
    decay_bias,
    rate_down,
    rate_up,
    rate_bias,
    head_gain,
    out_weight,
    memory_state,
    ffn_gain,
    blend_vector,
    dense_gate,
    dense_up,
    dense_down,
    expert_gate,
    expert_up,
    expert_down,
    routing,
    route_scale,
):
    seq_count, _ = hidden.shape
    kept, sent, new_state = attention(
        hidden,
        mix_gain,
        recept_weight,
        key_weight,
        value_weight,
        decay_down,
        decay_up,
        decay_bias,
        rate_down,
        rate_up,
        rate_bias,
        head_gain,
        out_weight,
        memory_state,
    )
    core = lax.axis_index("tp")
    half_rows = seq_count // 2
    chips = lax.axis_size("ep")
    dims = grid_of(chips)
    top_count = routing.shape[1]
    slot_cap = max(2, 2 * seq_count * top_count // chips)
    attn_sum = kept.astype(jnp.float32) + swap(sent).astype(jnp.float32)
    hidden_own = lax.dynamic_slice_in_dim(hidden, core * half_rows, half_rows, 0)
    first_res = (hidden_own.astype(jnp.float32) + attn_sum).astype(jnp.bfloat16)
    ffn_in = rms_scaled(first_res, ffn_gain).astype(jnp.bfloat16)
    notes = lax.dynamic_slice_in_dim(
        route_notes(routing, route_scale, chips), core * half_rows, half_rows, 0
    )
    rows = jnp.concatenate([ffn_in, notes], axis=1)

    near = dims[0] // 2
    line = [rows] + [hop(rows, dims, LINE, k) for k in range(1, dims[0])]
    chip = lax.axis_index("ep").astype(jnp.int32).reshape(1)
    weights = (
        expert_gate,
        expert_up,
        expert_down,
        dense_gate.T,
        dense_up.T,
        dense_down,
        blend_vector[None],
    )
    chip = touch(chip, *weights[:2])
    chip = touch(chip, *weights[2:6])
    sums = [first_res]
    for start in (0, near):
        own, other = plane_gather(jnp.stack(line[start : start + near]), dims)
        own, other = experts(own, other, slot_cap, half_rows, chip, weights)
        reduced = plane_reduce(own, other, dims)
        for k in range(near):
            if start + k:
                sums.append(hop(reduced[k], dims, LINE, -start - k))
            else:
                sums.append(reduced[k])
    out_own = total(*sums)
    out_other = swap(out_own)
    layer_out = jnp.concatenate(
        [jnp.where(core == 0, out_own, out_other), jnp.where(core == 0, out_other, out_own)]
    )
    return (layer_out, new_state)


def route_notes(routing, route_scale, chips):
    seq_count, top_count = routing.shape
    flat = routing.reshape(-1)
    one_hot = (flat[:, None] == jnp.arange(chips, dtype=jnp.int32)[None, :]).astype(jnp.int32)
    before = jnp.cumsum(one_hot, axis=0) - one_hot
    rank = jnp.sum(before * one_hot, axis=1).reshape(seq_count, top_count)
    high = route_scale.astype(jnp.bfloat16)
    low = (route_scale - high.astype(jnp.float32)).astype(jnp.bfloat16)
    fields = [routing.astype(jnp.bfloat16), rank.astype(jnp.bfloat16), high, low]
    notes = jnp.stack(fields, axis=2).reshape(seq_count, 4 * top_count)
    return jnp.pad(notes, ((0, 0), (0, 128 - 4 * top_count)))


def solution(mesh):
    in_specs = (
        P("ep", None),
        P(),
        P(None, "tp"),
        P(None, "tp"),
        P(None, "tp"),
        P(),
        P(),
        P(),
        P(),
        P(),
        P(),
        P(),
        P("tp", None),
        P("ep", "tp", None, None),
        P(),
        P(),
        P(None, ("ep", "tp")),
        P(None, ("ep", "tp")),
        P(("ep", "tp"), None),
        P("ep", None, "tp"),
        P("ep", None, "tp"),
        P("ep", "tp", None),
        P("ep", None),
        P("ep", None),
    )
    out_specs = (P("ep", None), P("ep", "tp", None, None))

    return jax.shard_map(shards, mesh=mesh, in_specs=in_specs, out_specs=out_specs, check_vma=False)
```

profile of v0, /device:TPU:0, one launch (start us, length us, event | category | flops | bytes accessed | tf_op | source)
XLA Modules:
  0.0 124.5 jit_solution(15840439487287575203)
XLA Ops:
  0.7 30.4 %attention.1 = (bf16[32,2048]{1,0:T(8,128)(2,1)}, bf16[32,2048]{1,0:T(8,128)(2,1)}, f32[64,8,64,64]{3,2,1,0:T(8,128)}) custom-call(s32[1]{0:T(128)} %bitcast.core_ref, bf16[64,2048]{1,0:T(8,128)(2,1)} %hidden_ref.1, f32[1,2048]{1,0:T(1,128)} %bitcast.96, bf16[2048,512]{1,0:T(8,128)(2,1)} %recept_ref.1, bf16[2048,512]{1,0:T(8,128)(2,1)} %key_ref.1, ...), custom_call_target="tpu_custom_call" | custom-call | tf_op jit(solution)/shard_map/attention/pallas_call | solution.py:315
  34.5 1.1 fusion.8
  35.8 4.7 %collective-permute-start.12 = (bf16[32,2176]{1,0:T(8,128)(2,1)S(1)}, bf16[32,2176]{1,0:T(8,128)(2,1)S(1)}, u32[]{:S(2)}, u32[]{:S(2)}) collective-permute-start(bf16[32,2176]{1,0:T(8,128)(2,1)S(1)} %get-tuple-element.35), channel_id=1, source_target_pairs={{0,24},{1,25},{2,26},{3,27},{4,28},{5,29},{6,30},{7,31},{8,0},{9,1... | collective-permute-start | bytes 417800 | tf_op jit(solution)/shard_map/ppermute | solution.py:150
  40.5 1.0 collective-permute-start.1
  41.5 3.1 %collective-permute-done.12 = bf16[32,2176]{1,0:T(8,128)(2,1)S(1)} collective-permute-done((bf16[32,2176]{1,0:T(8,128)(2,1)S(1)}, bf16[32,2176]{1,0:T(8,128)(2,1)S(1)}, u32[]{:S(2)}, u32[]{:S(2)}) %collective-permute-start.12) | collective-permute-done | bytes 139296 | tf_op jit(solution)/shard_map/ppermute | solution.py:150
  44.6 8.5 %collective-permute-done.11 = bf16[32,2176]{1,0:T(8,128)(2,1)S(1)} collective-permute-done((bf16[32,2176]{1,0:T(8,128)(2,1)S(1)}, bf16[32,2176]{1,0:T(8,128)(2,1)S(1)}, u32[]{:S(2)}, u32[]{:S(2)}) %collective-permute-start.11) | collective-permute-done | bytes 139296 | tf_op jit(solution)/shard_map/ppermute | solution.py:150
  53.2 1.6 %collective-permute-start.13 = (bf16[2,32,2176]{2,1,0:T(8,128)(2,1)S(1)}, bf16[2,32,2176]{2,1,0:T(8,128)(2,1)S(1)}, u32[]{:S(2)}, u32[]{:S(2)}) collective-permute-start(bf16[2,32,2176]{2,1,0:T(8,128)(2,1)S(1)} %get-tuple-element.29), channel_id=1, source_target_pairs={{0,2},{1,5},{2,0},{3,7},{4,6},{5,1},{6,4},{7,3},{8,10},{9,13},{10,... | collective-permute-start | bytes 835592 | tf_op jit(solution)/shard_map/ppermute | solution.py:150
  55.4 4.4 %collective-permute-done.13 = bf16[2,32,2176]{2,1,0:T(8,128)(2,1)S(1)} collective-permute-done((bf16[2,32,2176]{2,1,0:T(8,128)(2,1)S(1)}, bf16[2,32,2176]{2,1,0:T(8,128)(2,1)S(1)}, u32[]{:S(2)}, u32[]{:S(2)}) %collective-permute-start.13) | collective-permute-done | bytes 278560 | tf_op jit(solution)/shard_map/ppermute | solution.py:150
  59.8 0.9 pad_maximum_fusion.1
  60.7 1.5 %collective-permute-start.14 = (bf16[2,2,32,2176]{3,2,1,0:T(8,128)(2,1)}, bf16[2,2,32,2176]{3,2,1,0:T(8,128)(2,1)}, u32[]{:S(2)}, u32[]{:S(2)}) collective-permute-start(bf16[2,2,32,2176]{3,2,1,0:T(8,128)(2,1)} %pad_maximum_fusion.1), channel_id=1, source_target_pairs={{0,4},{1,3},{2,6},{3,1},{4,0},{5,7},{6,2},{7,5},{8,12},{9,11},{10,... | collective-permute-start | bytes 1671176 | tf_op jit(solution)/shard_map/ppermute | solution.py:150
  62.2 1.2 collective-permute-done.2
  63.4 0.9 pad_maximum_fusion
  64.2 1.5 %collective-permute-start.3 = (bf16[2,2,32,2176]{3,2,1,0:T(8,128)(2,1)}, bf16[2,2,32,2176]{3,2,1,0:T(8,128)(2,1)}, u32[]{:S(2)}, u32[]{:S(2)}) collective-permute-start(bf16[2,2,32,2176]{3,2,1,0:T(8,128)(2,1)} %pad_maximum_fusion), channel_id=1, source_target_pairs={{0,4},{1,3},{2,6},{3,1},{4,0},{5,7},{6,2},{7,5},{8,12},{9,11},{10,... | collective-permute-start | bytes 1671176 | tf_op jit(solution)/shard_map/ppermute | solution.py:150
  65.8 4.8 %collective-permute-done.14 = bf16[2,2,32,2176]{3,2,1,0:T(8,128)(2,1)} collective-permute-done((bf16[2,2,32,2176]{3,2,1,0:T(8,128)(2,1)}, bf16[2,2,32,2176]{3,2,1,0:T(8,128)(2,1)}, u32[]{:S(2)}, u32[]{:S(2)}) %collective-permute-start.14) | collective-permute-done | bytes 557088 | tf_op jit(solution)/shard_map/ppermute | solution.py:150
  70.6 1.9 %copy-done.2 = bf16[1,2048,768]{2,1,0:T(8,128)(2,1)S(1)} copy-done((bf16[1,2048,768]{2,1,0:T(8,128)(2,1)S(1)}, bf16[1,2048,768]{2,1,0:T(8,128)(2,1)}, u32[]{:S(2)}) %copy-start.2) | copy-done | bytes 3145752
  73.0 1.3 %copy-done = bf16[1,768,2048]{2,1,0:T(8,128)(2,1)S(1)} copy-done((bf16[1,768,2048]{2,1,0:T(8,128)(2,1)S(1)}, bf16[1,768,2048]{2,1,0:T(8,128)(2,1)}, u32[]{:S(2)}) %copy-start) | copy-done | bytes 3145752
  74.9 1.1 touch.3.chip_ref
  76.7 7.2 %experts.3 = (bf16[128,2048]{1,0:T(8,128)(2,1)S(1)}, bf16[128,2048]{1,0:T(8,128)(2,1)S(1)}, bf16[128,2048]{1,0:T(8,128)(2,1)S(1)}, bf16[128,2048]{1,0:T(8,128)(2,1)S(1)}) custom-call(s32[1]{0:T(128)} %touch.3.chip_ref, bf16[1,2048,768]{2,1,0:T(8,128)(2,1)S(1)} %copy-done.1, bf16[1,2048,768]{2,1,0:T(8,128)(2,1)S(1)} %copy-done.3, ...), custom_call_target="tpu_custom_call" | custom-call | flops 9663676416 | bytes 9437184 | tf_op jit(solution)/shard_map/experts/pallas_call | solution.py:111
  84.4 6.8 %experts.2 = (bf16[128,2048]{1,0:T(8,128)(2,1)S(1)}, bf16[128,2048]{1,0:T(8,128)(2,1)S(1)}, bf16[128,2048]{1,0:T(8,128)(2,1)S(1)}, bf16[128,2048]{1,0:T(8,128)(2,1)S(1)}) custom-call(s32[1]{0:T(128)} %touch.3.chip_ref, bf16[1,2048,768]{2,1,0:T(8,128)(2,1)S(1)} %copy-done.1, bf16[1,2048,768]{2,1,0:T(8,128)(2,1)S(1)} %copy-done.3, ...), custom_call_target="tpu_custom_call" | custom-call | flops 9663676416 | bytes 9437184 | tf_op jit(solution)/shard_map/experts/pallas_call | solution.py:111
  92.0 1.6 %collective-permute-start.19 = (bf16[2,2,32,2048]{3,2,1,0:T(8,128)(2,1)S(1)}, bf16[2,2,32,2048]{3,2,1,0:T(8,128)(2,1)S(1)}, u32[]{:S(2)}, u32[]{:S(2)}) collective-permute-start(bf16[2,2,32,2048]{3,2,1,0:T(8,128)(2,1)S(1)} %fusion), channel_id=1, source_target_pairs={{0,4},{1,3},{2,6},{3,1},{4,0},{5,7},{6,2},{7,5},{8,12},{9,11},{10,... | collective-permute-start | bytes 1572872 | tf_op jit(solution)/shard_map/ppermute | solution.py:150
  93.7 1.4 %collective-permute-start.8 = (bf16[2,2,32,2048]{3,2,1,0:T(8,128)(2,1)S(1)}, bf16[2,2,32,2048]{3,2,1,0:T(8,128)(2,1)S(1)}, u32[]{:S(2)}, u32[]{:S(2)}) collective-permute-start(bf16[2,2,32,2048]{3,2,1,0:T(8,128)(2,1)S(1)} %fusion.3), channel_id=1, source_target_pairs={{0,4},{1,3},{2,6},{3,1},{4,0},{5,7},{6,2},{7,5},{8,12},{9,11},{10,... | collective-permute-start | bytes 1572872 | tf_op jit(solution)/shard_map/ppermute | solution.py:150
  95.1 6.2 %collective-permute-done.19 = bf16[2,2,32,2048]{3,2,1,0:T(8,128)(2,1)S(1)} collective-permute-done((bf16[2,2,32,2048]{3,2,1,0:T(8,128)(2,1)S(1)}, bf16[2,2,32,2048]{3,2,1,0:T(8,128)(2,1)S(1)}, u32[]{:S(2)}, u32[]{:S(2)}) %collective-permute-start.19) | collective-permute-done | bytes 524320 | tf_op jit(solution)/shard_map/ppermute | solution.py:150
  101.5 1.6 %collective-permute-start.20 = (bf16[2,32,2048]{2,1,0:T(8,128)(2,1)S(1)}, bf16[2,32,2048]{2,1,0:T(8,128)(2,1)S(1)}, u32[]{:S(2)}, u32[]{:S(2)}) collective-permute-start(bf16[2,32,2048]{2,1,0:T(8,128)(2,1)S(1)} %slice_bitcast_fusion), channel_id=1, source_target_pairs={{0,2},{1,5},{2,0},{3,7},{4,6},{5,1},{6,4},{7,3},{8,10},{9,13},{10,... | collective-permute-start | bytes 786440 | tf_op jit(solution)/shard_map/ppermute | solution.py:150
  103.1 6.6 %collective-permute-done.8 = bf16[2,2,32,2048]{3,2,1,0:T(8,128)(2,1)S(1)} collective-permute-done((bf16[2,2,32,2048]{3,2,1,0:T(8,128)(2,1)S(1)}, bf16[2,2,32,2048]{3,2,1,0:T(8,128)(2,1)S(1)}, u32[]{:S(2)}, u32[]{:S(2)}) %collective-permute-start.8) | collective-permute-done | bytes 524320 | tf_op jit(solution)/shard_map/ppermute | solution.py:150
  109.9 1.6 %collective-permute-start.9 = (bf16[2,32,2048]{2,1,0:T(8,128)(2,1)S(1)}, bf16[2,32,2048]{2,1,0:T(8,128)(2,1)S(1)}, u32[]{:S(2)}, u32[]{:S(2)}) collective-permute-start(bf16[2,32,2048]{2,1,0:T(8,128)(2,1)S(1)} %slice_bitcast_fusion.2), channel_id=1, source_target_pairs={{0,2},{1,5},{2,0},{3,7},{4,6},{5,1},{6,4},{7,3},{8,10},{9,13},{10,... | collective-permute-start | bytes 786440 | tf_op jit(solution)/shard_map/ppermute | solution.py:150
  111.7 1.8 %collective-permute-start.21 = (bf16[32,2048]{1,0:T(8,128)(2,1)S(1)}, bf16[32,2048]{1,0:T(8,128)(2,1)S(1)}, u32[]{:S(2)}, u32[]{:S(2)}) collective-permute-start(bf16[32,2048]{1,0:T(8,128)(2,1)S(1)} %get-tuple-element.32), channel_id=1, source_target_pairs={{0,16},{1,17},{2,18},{3,19},{4,20},{5,21},{6,22},{7,23},{8,24},{9,... | collective-permute-start | bytes 393224 | tf_op jit(solution)/shard_map/ppermute | solution.py:150
  113.4 2.9 %collective-permute-done.9 = bf16[2,32,2048]{2,1,0:T(8,128)(2,1)S(1)} collective-permute-done((bf16[2,32,2048]{2,1,0:T(8,128)(2,1)S(1)}, bf16[2,32,2048]{2,1,0:T(8,128)(2,1)S(1)}, u32[]{:S(2)}, u32[]{:S(2)}) %collective-permute-start.9) | collective-permute-done | bytes 262176 | tf_op jit(solution)/shard_map/ppermute | solution.py:150
  116.5 1.3 %collective-permute-start.10 = (bf16[32,2048]{1,0:T(8,128)(2,1)S(1)}, bf16[32,2048]{1,0:T(8,128)(2,1)S(1)}, u32[]{:S(2)}, u32[]{:S(2)}) collective-permute-start(bf16[32,2048]{1,0:T(8,128)(2,1)S(1)} %slice_bitcast_fusion.6), channel_id=1, source_target_pairs={{0,24},{1,25},{2,26},{3,27},{4,28},{5,29},{6,30},{7,31},{8,0},{9,1... | collective-permute-start | bytes 393224 | tf_op jit(solution)/shard_map/ppermute | solution.py:150
  117.7 1.6 %collective-permute-done.22 = bf16[32,2048]{1,0:T(8,128)(2,1)S(1)} collective-permute-done((bf16[32,2048]{1,0:T(8,128)(2,1)S(1)}, bf16[32,2048]{1,0:T(8,128)(2,1)S(1)}, u32[]{:S(2)}, u32[]{:S(2)}) %collective-permute-start.22) | collective-permute-done | bytes 131104 | tf_op jit(solution)/shard_map/ppermute | solution.py:150
  119.3 2.9 %collective-permute-done.21 = bf16[32,2048]{1,0:T(8,128)(2,1)S(1)} collective-permute-done((bf16[32,2048]{1,0:T(8,128)(2,1)S(1)}, bf16[32,2048]{1,0:T(8,128)(2,1)S(1)}, u32[]{:S(2)}, u32[]{:S(2)}) %collective-permute-start.21) | collective-permute-done | bytes 131104 | tf_op jit(solution)/shard_map/ppermute | solution.py:150
  122.4 1.3 %collective-permute-done.23 = bf16[32,2048]{1,0:T(8,128)(2,1)S(1)} collective-permute-done((bf16[32,2048]{1,0:T(8,128)(2,1)S(1)}, bf16[32,2048]{1,0:T(8,128)(2,1)S(1)}, u32[]{:S(2)}, u32[]{:S(2)}) %collective-permute-start.23) | collective-permute-done | bytes 131104 | tf_op jit(solution)/shard_map/ppermute | solution.py:154
  123.7 0.7 pad_maximum_fusion.4
  (81 shorter events, 8.4 us)
Async XLA Ops:
  0.6 31.0 %copy-start.10 = (s32[64,2]{0,1:T(2,128)S(1)}, s32[64,2]{0,1:T(2,128)}, u32[]{:S(2)}) copy-start(s32[64,2]{0,1:T(2,128)} %param.46) | copy-start | bytes 1540
  0.7 31.6 %copy-start.11 = (f32[64,2]{0,1:T(2,128)S(1)}, f32[64,2]{0,1:T(2,128)}, u32[]{:S(2)}) copy-start(f32[64,2]{0,1:T(2,128)} %param.47) | copy-start | bytes 1540
  0.7 33.9 %copy-start.7 = (bf16[64,2048]{1,0:T(8,128)(2,1)S(1)}, bf16[64,2048]{1,0:T(8,128)(2,1)}, u32[]{:S(2)}) copy-start(bf16[64,2048]{1,0:T(8,128)(2,1)} %hidden_ref.1) | copy-start | bytes 786436
  0.7 35.0 %copy-start.8 = (f32[2048]{0:T(1024)S(1)}, f32[2048]{0:T(1024)}, u32[]{:S(2)}) copy-start(f32[2048]{0:T(1024)} %param.38) | copy-start | bytes 24580
  31.0 39.5 %copy-start.9 = (bf16[2048]{0:T(1024)(128)(2,1)S(1)}, bf16[2048]{0:T(1024)(128)(2,1)}, u32[]{:S(2)}) copy-start(bf16[2048]{0:T(1024)(128)(2,1)} %param.39) | copy-start | bytes 12292
  31.0 39.5 %copy-start.1 = (bf16[1,2048,768]{2,1,0:T(8,128)(2,1)S(1)}, bf16[1,2048,768]{2,1,0:T(8,128)(2,1)}, u32[]{:S(2)}) copy-start(bf16[1,2048,768]{2,1,0:T(8,128)(2,1)} %expert_gate_ref.3) | copy-start | bytes 9437188
  31.1 3.5 %collective-permute-start = (bf16[32,2048]{1,0:T(8,128)(2,1)}, bf16[32,2048]{1,0:T(8,128)(2,1)}, u32[]{:S(2)}, u32[]{:S(2)}) collective-permute-start(bf16[32,2048]{1,0:T(8,128)(2,1)} %get-tuple-element.14), channel_id=1, source_target_pairs={{0,1},{1,0},{2,3},{3,2},{4,5},{5,4},{6,7},{7,6},{8,9},{9,8},{10,11... | collective-permute-start | bytes 393224 | tf_op jit(solution)/shard_map/ppermute | solution.py:154
  35.8 8.8 %collective-permute-start.12 = (bf16[32,2176]{1,0:T(8,128)(2,1)S(1)}, bf16[32,2176]{1,0:T(8,128)(2,1)S(1)}, u32[]{:S(2)}, u32[]{:S(2)}) collective-permute-start(bf16[32,2176]{1,0:T(8,128)(2,1)S(1)} %get-tuple-element.35), channel_id=1, source_target_pairs={{0,24},{1,25},{2,26},{3,27},{4,28},{5,29},{6,30},{7,31},{8,0},{9,1... | collective-permute-start | bytes 417800 | tf_op jit(solution)/shard_map/ppermute | solution.py:150
  40.5 12.7 %collective-permute-start.11 = (bf16[32,2176]{1,0:T(8,128)(2,1)S(1)}, bf16[32,2176]{1,0:T(8,128)(2,1)S(1)}, u32[]{:S(2)}, u32[]{:S(2)}) collective-permute-start(bf16[32,2176]{1,0:T(8,128)(2,1)S(1)} %get-tuple-element.35), channel_id=1, source_target_pairs={{0,16},{1,17},{2,18},{3,19},{4,20},{5,21},{6,22},{7,23},{8,24},{9,... | collective-permute-start | bytes 417800 | tf_op jit(solution)/shard_map/ppermute | solution.py:150
  40.5 14.3 %collective-permute-start.1 = (bf16[32,2176]{1,0:T(8,128)(2,1)S(1)}, bf16[32,2176]{1,0:T(8,128)(2,1)S(1)}, u32[]{:S(2)}, u32[]{:S(2)}) collective-permute-start(bf16[32,2176]{1,0:T(8,128)(2,1)S(1)} %get-tuple-element.35), channel_id=1, source_target_pairs={{0,8},{1,9},{2,10},{3,11},{4,12},{5,13},{6,14},{7,15},{8,16},{9,17... | collective-permute-start | bytes 417800 | tf_op jit(solution)/shard_map/ppermute | solution.py:150
  53.2 6.6 %collective-permute-start.13 = (bf16[2,32,2176]{2,1,0:T(8,128)(2,1)S(1)}, bf16[2,32,2176]{2,1,0:T(8,128)(2,1)S(1)}, u32[]{:S(2)}, u32[]{:S(2)}) collective-permute-start(bf16[2,32,2176]{2,1,0:T(8,128)(2,1)S(1)} %get-tuple-element.29), channel_id=1, source_target_pairs={{0,2},{1,5},{2,0},{3,7},{4,6},{5,1},{6,4},{7,3},{8,10},{9,13},{10,... | collective-permute-start | bytes 835592 | tf_op jit(solution)/shard_map/ppermute | solution.py:150
  54.8 8.6 %collective-permute-start.2 = (bf16[2,32,2176]{2,1,0:T(8,128)(2,1)S(1)}, bf16[2,32,2176]{2,1,0:T(8,128)(2,1)S(1)}, u32[]{:S(2)}, u32[]{:S(2)}) collective-permute-start(bf16[2,32,2176]{2,1,0:T(8,128)(2,1)S(1)} %get-tuple-element.27), channel_id=1, source_target_pairs={{0,2},{1,5},{2,0},{3,7},{4,6},{5,1},{6,4},{7,3},{8,10},{9,13},{10,... | collective-permute-start | bytes 835592 | tf_op jit(solution)/shard_map/ppermute | solution.py:150
  60.7 9.8 %collective-permute-start.14 = (bf16[2,2,32,2176]{3,2,1,0:T(8,128)(2,1)}, bf16[2,2,32,2176]{3,2,1,0:T(8,128)(2,1)}, u32[]{:S(2)}, u32[]{:S(2)}) collective-permute-start(bf16[2,2,32,2176]{3,2,1,0:T(8,128)(2,1)} %pad_maximum_fusion.1), channel_id=1, source_target_pairs={{0,4},{1,3},{2,6},{3,1},{4,0},{5,7},{6,2},{7,5},{8,12},{9,11},{10,... | collective-permute-start | bytes 1671176 | tf_op jit(solution)/shard_map/ppermute | solution.py:150
  64.2 12.4 %collective-permute-start.3 = (bf16[2,2,32,2176]{3,2,1,0:T(8,128)(2,1)}, bf16[2,2,32,2176]{3,2,1,0:T(8,128)(2,1)}, u32[]{:S(2)}, u32[]{:S(2)}) collective-permute-start(bf16[2,2,32,2176]{3,2,1,0:T(8,128)(2,1)} %pad_maximum_fusion), channel_id=1, source_target_pairs={{0,4},{1,3},{2,6},{3,1},{4,0},{5,7},{6,2},{7,5},{8,12},{9,11},{10,... | collective-permute-start | bytes 1671176 | tf_op jit(solution)/shard_map/ppermute | solution.py:150
  65.8 11.0 %collective-permute-start.15 = (bf16[2,2,32,2176]{3,2,1,0:T(8,128)(2,1)}, bf16[2,2,32,2176]{3,2,1,0:T(8,128)(2,1)}, u32[]{:S(2)}, u32[]{:S(2)}) collective-permute-start(bf16[2,2,32,2176]{3,2,1,0:T(8,128)(2,1)} %pad_maximum_fusion.1), channel_id=1, source_target_pairs={{0,1},{1,0},{2,3},{3,2},{4,5},{5,4},{6,7},{7,6},{8,9},{9,8},{10,11... | collective-permute-start | bytes 1671176 | tf_op jit(solution)/shard_map/ppermute | solution.py:154
  70.5 6.2 %collective-permute-start.16 = (bf16[2,2,32,2176]{3,2,1,0:T(8,128)(2,1)}, bf16[2,2,32,2176]{3,2,1,0:T(8,128)(2,1)}, u32[]{:S(2)}, u32[]{:S(2)}) collective-permute-start(bf16[2,2,32,2176]{3,2,1,0:T(8,128)(2,1)} %collective-permute-done.14), channel_id=1, source_target_pairs={{0,1},{1,0},{2,3},{3,2},{4,5},{5,4},{6,7},{7,6},{8,9},{9,8},{10,11... | collective-permute-start | bytes 1671176 | tf_op jit(solution)/shard_map/ppermute | solution.py:154
  72.4 2.5 %copy-start.6 = (bf16[176,2048]{1,0:T(8,128)(2,1)S(1)}, bf16[176,2048]{1,0:T(8,128)(2,1)}, u32[]{:S(2)}) copy-start(bf16[176,2048]{1,0:T(8,128)(2,1)} %dense_down_ref.3) | copy-start | bytes 2162692
  73.0 3.8 %copy-start.3 = (bf16[1,2048,768]{2,1,0:T(8,128)(2,1)S(1)}, bf16[1,2048,768]{2,1,0:T(8,128)(2,1)}, u32[]{:S(2)}) copy-start(bf16[1,2048,768]{2,1,0:T(8,128)(2,1)} %expert_up_ref.3) | copy-start | bytes 9437188
  76.1 8.3 %collective-permute-start.4 = (bf16[2,2,32,2176]{3,2,1,0:T(8,128)(2,1)}, bf16[2,2,32,2176]{3,2,1,0:T(8,128)(2,1)S(1)}, u32[]{:S(2)}, u32[]{:S(2)}) collective-permute-start(bf16[2,2,32,2176]{3,2,1,0:T(8,128)(2,1)} %pad_maximum_fusion), channel_id=1, source_target_pairs={{0,1},{1,0},{2,3},{3,2},{4,5},{5,4},{6,7},{7,6},{8,9},{9,8},{10,11... | collective-permute-start | bytes 1671176 | tf_op jit(solution)/shard_map/ppermute | solution.py:154
  76.7 7.8 %collective-permute-start.5 = (bf16[2,2,32,2176]{3,2,1,0:T(8,128)(2,1)}, bf16[2,2,32,2176]{3,2,1,0:T(8,128)(2,1)S(1)}, u32[]{:S(2)}, u32[]{:S(2)}) collective-permute-start(bf16[2,2,32,2176]{3,2,1,0:T(8,128)(2,1)} %collective-permute-done.3), channel_id=1, source_target_pairs={{0,1},{1,0},{2,3},{3,2},{4,5},{5,4},{6,7},{7,6},{8,9},{9,8},{10,11... | collective-permute-start | bytes 1671176 | tf_op jit(solution)/shard_map/ppermute | solution.py:154
  83.9 7.9 %collective-permute-start.18 = (bf16[2,2,32,2048]{3,2,1,0:T(8,128)(2,1)S(1)}, bf16[2,2,32,2048]{3,2,1,0:T(8,128)(2,1)S(1)}, u32[]{:S(2)}, u32[]{:S(2)}) collective-permute-start(bf16[2,2,32,2048]{3,2,1,0:T(8,128)(2,1)S(1)} %bitcast.87), channel_id=1, source_target_pairs={{0,1},{1,0},{2,3},{3,2},{4,5},{5,4},{6,7},{7,6},{8,9},{9,8},{10,11... | collective-permute-start | bytes 1572872 | tf_op jit(solution)/shard_map/ppermute | solution.py:154
  91.3 2.3 %collective-permute-start.7 = (bf16[2,2,32,2048]{3,2,1,0:T(8,128)(2,1)S(1)}, bf16[2,2,32,2048]{3,2,1,0:T(8,128)(2,1)S(1)}, u32[]{:S(2)}, u32[]{:S(2)}) collective-permute-start(bf16[2,2,32,2048]{3,2,1,0:T(8,128)(2,1)S(1)} %bitcast.88), channel_id=1, source_target_pairs={{0,1},{1,0},{2,3},{3,2},{4,5},{5,4},{6,7},{7,6},{8,9},{9,8},{10,11... | collective-permute-start | bytes 1572872 | tf_op jit(solution)/shard_map/ppermute | solution.py:154
  91.4 3.6 %collective-permute-start.17 = (bf16[2,2,32,2048]{3,2,1,0:T(8,128)(2,1)S(1)}, bf16[2,2,32,2048]{3,2,1,0:T(8,128)(2,1)S(1)}, u32[]{:S(2)}, u32[]{:S(2)}) collective-permute-start(bf16[2,2,32,2048]{3,2,1,0:T(8,128)(2,1)S(1)} %bitcast.85), channel_id=1, source_target_pairs={{0,1},{1,0},{2,3},{3,2},{4,5},{5,4},{6,7},{7,6},{8,9},{9,8},{10,11... | collective-permute-start | bytes 1572872 | tf_op jit(solution)/shard_map/ppermute | solution.py:154
  92.0 9.2 %collective-permute-start.19 = (bf16[2,2,32,2048]{3,2,1,0:T(8,128)(2,1)S(1)}, bf16[2,2,32,2048]{3,2,1,0:T(8,128)(2,1)S(1)}, u32[]{:S(2)}, u32[]{:S(2)}) collective-permute-start(bf16[2,2,32,2048]{3,2,1,0:T(8,128)(2,1)S(1)} %fusion), channel_id=1, source_target_pairs={{0,4},{1,3},{2,6},{3,1},{4,0},{5,7},{6,2},{7,5},{8,12},{9,11},{10,... | collective-permute-start | bytes 1572872 | tf_op jit(solution)/shard_map/ppermute | solution.py:150
  93.6 9.5 %collective-permute-start.6 = (bf16[2,2,32,2048]{3,2,1,0:T(8,128)(2,1)S(1)}, bf16[2,2,32,2048]{3,2,1,0:T(8,128)(2,1)S(1)}, u32[]{:S(2)}, u32[]{:S(2)}) collective-permute-start(bf16[2,2,32,2048]{3,2,1,0:T(8,128)(2,1)S(1)} %bitcast.86), channel_id=1, source_target_pairs={{0,1},{1,0},{2,3},{3,2},{4,5},{5,4},{6,7},{7,6},{8,9},{9,8},{10,11... | collective-permute-start | bytes 1572872 | tf_op jit(solution)/shard_map/ppermute | solution.py:154
  93.7 15.9 %collective-permute-start.8 = (bf16[2,2,32,2048]{3,2,1,0:T(8,128)(2,1)S(1)}, bf16[2,2,32,2048]{3,2,1,0:T(8,128)(2,1)S(1)}, u32[]{:S(2)}, u32[]{:S(2)}) collective-permute-start(bf16[2,2,32,2048]{3,2,1,0:T(8,128)(2,1)S(1)} %fusion.3), channel_id=1, source_target_pairs={{0,4},{1,3},{2,6},{3,1},{4,0},{5,7},{6,2},{7,5},{8,12},{9,11},{10,... | collective-permute-start | bytes 1572872 | tf_op jit(solution)/shard_map/ppermute | solution.py:150
  101.5 10.0 %collective-permute-start.20 = (bf16[2,32,2048]{2,1,0:T(8,128)(2,1)S(1)}, bf16[2,32,2048]{2,1,0:T(8,128)(2,1)S(1)}, u32[]{:S(2)}, u32[]{:S(2)}) collective-permute-start(bf16[2,32,2048]{2,1,0:T(8,128)(2,1)S(1)} %slice_bitcast_fusion), channel_id=1, source_target_pairs={{0,2},{1,5},{2,0},{3,7},{4,6},{5,1},{6,4},{7,3},{8,10},{9,13},{10,... | collective-permute-start | bytes 786440 | tf_op jit(solution)/shard_map/ppermute | solution.py:150
  109.9 6.4 %collective-permute-start.9 = (bf16[2,32,2048]{2,1,0:T(8,128)(2,1)S(1)}, bf16[2,32,2048]{2,1,0:T(8,128)(2,1)S(1)}, u32[]{:S(2)}, u32[]{:S(2)}) collective-permute-start(bf16[2,32,2048]{2,1,0:T(8,128)(2,1)S(1)} %slice_bitcast_fusion.2), channel_id=1, source_target_pairs={{0,2},{1,5},{2,0},{3,7},{4,6},{5,1},{6,4},{7,3},{8,10},{9,13},{10,... | collective-permute-start | bytes 786440 | tf_op jit(solution)/shard_map/ppermute | solution.py:150
  111.6 7.7 %collective-permute-start.22 = (bf16[32,2048]{1,0:T(8,128)(2,1)S(1)}, bf16[32,2048]{1,0:T(8,128)(2,1)S(1)}, u32[]{:S(2)}, u32[]{:S(2)}) collective-permute-start(bf16[32,2048]{1,0:T(8,128)(2,1)S(1)} %get-tuple-element.33), channel_id=1, source_target_pairs={{0,8},{1,9},{2,10},{3,11},{4,12},{5,13},{6,14},{7,15},{8,16},{9,17... | collective-permute-start | bytes 393224 | tf_op jit(solution)/shard_map/ppermute | solution.py:150
  111.7 10.5 %collective-permute-start.21 = (bf16[32,2048]{1,0:T(8,128)(2,1)S(1)}, bf16[32,2048]{1,0:T(8,128)(2,1)S(1)}, u32[]{:S(2)}, u32[]{:S(2)}) collective-permute-start(bf16[32,2048]{1,0:T(8,128)(2,1)S(1)} %get-tuple-element.32), channel_id=1, source_target_pairs={{0,16},{1,17},{2,18},{3,19},{4,20},{5,21},{6,22},{7,23},{8,24},{9,... | collective-permute-start | bytes 393224 | tf_op jit(solution)/shard_map/ppermute | solution.py:150
  116.5 5.8 %collective-permute-start.10 = (bf16[32,2048]{1,0:T(8,128)(2,1)S(1)}, bf16[32,2048]{1,0:T(8,128)(2,1)S(1)}, u32[]{:S(2)}, u32[]{:S(2)}) collective-permute-start(bf16[32,2048]{1,0:T(8,128)(2,1)S(1)} %slice_bitcast_fusion.6), channel_id=1, source_target_pairs={{0,24},{1,25},{2,26},{3,27},{4,28},{5,29},{6,30},{7,31},{8,0},{9,1... | collective-permute-start | bytes 393224 | tf_op jit(solution)/shard_map/ppermute | solution.py:150
  122.3 1.4 %collective-permute-start.23 = (bf16[32,2048]{1,0:T(8,128)(2,1)S(1)}, bf16[32,2048]{1,0:T(8,128)(2,1)S(1)}, u32[]{:S(2)}, u32[]{:S(2)}) collective-permute-start(bf16[32,2048]{1,0:T(8,128)(2,1)S(1)} %fusion.14), channel_id=1, source_target_pairs={{0,1},{1,0},{2,3},{3,2},{4,5},{5,4},{6,7},{7,6},{8,9},{9,8},{10,11... | collective-permute-start | bytes 393224 | tf_op jit(solution)/shard_map/ppermute | solution.py:154
  (4 other events, 8.1 us)
where the time goes:
time: 125 us; the launch traced here: 124 us
  Pallas kernels  46 us (37%)
  waiting for transfers between devices  43.5 us (35%)
  starting transfers between devices  22.4 us (18%)
  other arithmetic  7.03 us (6%)
  local copies, waits for them, and re-layouts  4.53 us (4%)
    ppermute x14, waiting for transfers between devices, hop(): return lax.ppermute(value, ('ep', 'tp'), perm)  42.1 us
    pallas_call x1, Pallas kernels, attention(): pl.pallas_call(attention_kernel, grid_spec=pltpu.PrefetchScalarGridSpec(n...  30.4 us
    ppermute x14, starting transfers between devices, hop(): return lax.ppermute(value, ('ep', 'tp'), perm)  20.1 us
    pallas_call x2, Pallas kernels, experts(): pl.pallas_call(functools.partial(experts_kernel, tuple(pieces), cap, span...  14 us
    unnamed x25, local copies, waits for them, and re-layouts  3.97 us
  transfers between devices with their start and end apart: 24, of which 11 were waited for; matrix products, arithmetic and copies ran while one was open for 4% of the time, Pallas kernels for 13%

commit v1 on v0

--- a/solution.py
+++ b/solution.py
@@ -242,13 +242,16 @@
     rows = pl.ds(pl.multiple_of(step * block, block), block)
     ones = jnp.ones((size, 128), jnp.bfloat16)
     lane = lax.broadcasted_iota(jnp.int32, (size, 128), 1)
-    for head in range(heads):
+
+    def pulled(head):
         unit = unit_scr[head, rows, :]
         products = [
             (state_ref[seq, head] * unit[seq : seq + 1]).astype(jnp.bfloat16)
             for seq in range(block)
         ]
-        removed = matmul(jnp.concatenate(products), ones)
+        return matmul(jnp.concatenate(products), ones)
+
+    def updated(head, removed):
         pull = pull_scr[head, rows, :]
         push = push_scr[head, rows, :]
         decay = decay_scr[head, rows, :]
@@ -264,7 +267,9 @@
             )
             new_ref[seq, head] = fresh
             products.append((fresh * recept[one]).astype(jnp.bfloat16))
-        readout = matmul(jnp.concatenate(products), ones)
+        return matmul(jnp.concatenate(products), ones)
+
+    def normed(head, readout):
         columns = jnp.zeros((size, 128), jnp.float32)
         for seq in range(block):
             columns = jnp.where(lane == seq, readout[seq * size : (seq + 1) * size], columns)
@@ -276,6 +281,16 @@
             * lax.rsqrt(variance + 0.00064)
             * gain_ref[:, head * size : (head + 1) * size]
         )
+
+    removed = pulled(0)
+    readout = None
+    for head in range(heads):
+        following = pulled(head + 1) if head + 1 < heads else None
+        finished = updated(head, removed)
+        if head:
+            normed(head - 1, readout)
+        removed, readout = following, finished
+    normed(heads - 1, readout)
 
     @pl.when(step == pl.num_programs(0) - 1)
     def _():

time: 125 us -> 121 us (0.968)
  Pallas kernels: 46 us -> 42 us
    pallas_call x1, Pallas kernels: 30.4 us -> 26.4 us  [attention(): pl.pallas_call(attention_kernel, grid_spec=pltpu.PrefetchScalarGridSpec(n...]
  transfers between devices with their start and end apart: 24 -> 24, of which waited for: 11 -> 11; matrix products, arithmetic and copies ran while one was open for 4% -> 5% of each run, Pallas kernels for 13% -> 13%
where the time goes in v1:
time: 121 us; the launch traced here: 120 us
  waiting for transfers between devices  43.4 us (36%)
  Pallas kernels  42 us (35%)
  starting transfers between devices  22.5 us (19%)
  other arithmetic  7.03 us (6%)
  local copies, waits for them, and re-layouts  4.53 us (4%)
    ppermute x14, waiting for transfers between devices, hop(): return lax.ppermute(value, ('ep', 'tp'), perm)  42.1 us
    pallas_call x1, Pallas kernels, attention(): pl.pallas_call(attention_kernel, grid_spec=pltpu.PrefetchScalarGridSpec(n...  26.4 us
    ppermute x14, starting transfers between devices, hop(): return lax.ppermute(value, ('ep', 'tp'), perm)  20.1 us
    pallas_call x2, Pallas kernels, experts(): pl.pallas_call(functools.partial(experts_kernel, tuple(pieces), cap, span...  14 us
    unnamed x25, local copies, waits for them, and re-layouts  3.97 us
  transfers between devices with their start and end apart: 24, of which 11 were waited for; matrix products, arithmetic and copies ran while one was open for 5% of the time, Pallas kernels for 13%

profile of v1, /device:TPU:0, one launch (start us, length us, event | category | flops | bytes accessed | tf_op | source)
XLA Modules:
  0.0 120.5 jit_solution(17557548968273139133)
XLA Ops:
  0.7 26.4 %attention.1 = (bf16[32,2048]{1,0:T(8,128)(2,1)}, bf16[32,2048]{1,0:T(8,128)(2,1)}, f32[64,8,64,64]{3,2,1,0:T(8,128)}) custom-call(s32[1]{0:T(128)} %bitcast.core_ref, bf16[64,2048]{1,0:T(8,128)(2,1)} %hidden_ref.1, f32[1,2048]{1,0:T(1,128)} %bitcast.96, bf16[2048,512]{1,0:T(8,128)(2,1)} %recept_ref.1, bf16[2048,512]{1,0:T(8,128)(2,1)} %key_ref.1, ...), custom_call_target="tpu_custom_call" | custom-call | tf_op jit(solution)/shard_map/attention/pallas_call | solution.py:330
  30.5 1.1 fusion.8
  31.8 4.7 %collective-permute-start.12 = (bf16[32,2176]{1,0:T(8,128)(2,1)S(1)}, bf16[32,2176]{1,0:T(8,128)(2,1)S(1)}, u32[]{:S(2)}, u32[]{:S(2)}) collective-permute-start(bf16[32,2176]{1,0:T(8,128)(2,1)S(1)} %get-tuple-element.35), channel_id=1, source_target_pairs={{0,24},{1,25},{2,26},{3,27},{4,28},{5,29},{6,30},{7,31},{8,0},{9,1... | collective-permute-start | bytes 417800 | tf_op jit(solution)/shard_map/ppermute | solution.py:150
  36.5 1.0 collective-permute-start.1
  37.5 3.1 %collective-permute-done.12 = bf16[32,2176]{1,0:T(8,128)(2,1)S(1)} collective-permute-done((bf16[32,2176]{1,0:T(8,128)(2,1)S(1)}, bf16[32,2176]{1,0:T(8,128)(2,1)S(1)}, u32[]{:S(2)}, u32[]{:S(2)}) %collective-permute-start.12) | collective-permute-done | bytes 139296 | tf_op jit(solution)/shard_map/ppermute | solution.py:150
  40.7 8.5 %collective-permute-done.11 = bf16[32,2176]{1,0:T(8,128)(2,1)S(1)} collective-permute-done((bf16[32,2176]{1,0:T(8,128)(2,1)S(1)}, bf16[32,2176]{1,0:T(8,128)(2,1)S(1)}, u32[]{:S(2)}, u32[]{:S(2)}) %collective-permute-start.11) | collective-permute-done | bytes 139296 | tf_op jit(solution)/shard_map/ppermute | solution.py:150
  49.2 1.6 %collective-permute-start.13 = (bf16[2,32,2176]{2,1,0:T(8,128)(2,1)S(1)}, bf16[2,32,2176]{2,1,0:T(8,128)(2,1)S(1)}, u32[]{:S(2)}, u32[]{:S(2)}) collective-permute-start(bf16[2,32,2176]{2,1,0:T(8,128)(2,1)S(1)} %get-tuple-element.29), channel_id=1, source_target_pairs={{0,2},{1,5},{2,0},{3,7},{4,6},{5,1},{6,4},{7,3},{8,10},{9,13},{10,... | collective-permute-start | bytes 835592 | tf_op jit(solution)/shard_map/ppermute | solution.py:150
  51.4 4.4 %collective-permute-done.13 = bf16[2,32,2176]{2,1,0:T(8,128)(2,1)S(1)} collective-permute-done((bf16[2,32,2176]{2,1,0:T(8,128)(2,1)S(1)}, bf16[2,32,2176]{2,1,0:T(8,128)(2,1)S(1)}, u32[]{:S(2)}, u32[]{:S(2)}) %collective-permute-start.13) | collective-permute-done | bytes 278560 | tf_op jit(solution)/shard_map/ppermute | solution.py:150
  55.8 0.9 pad_maximum_fusion.1
  56.7 1.5 %collective-permute-start.14 = (bf16[2,2,32,2176]{3,2,1,0:T(8,128)(2,1)}, bf16[2,2,32,2176]{3,2,1,0:T(8,128)(2,1)}, u32[]{:S(2)}, u32[]{:S(2)}) collective-permute-start(bf16[2,2,32,2176]{3,2,1,0:T(8,128)(2,1)} %pad_maximum_fusion.1), channel_id=1, source_target_pairs={{0,4},{1,3},{2,6},{3,1},{4,0},{5,7},{6,2},{7,5},{8,12},{9,11},{10,... | collective-permute-start | bytes 1671176 | tf_op jit(solution)/shard_map/ppermute | solution.py:150
  58.2 1.2 collective-permute-done.2
  59.4 0.9 pad_maximum_fusion
  60.2 1.5 %collective-permute-start.3 = (bf16[2,2,32,2176]{3,2,1,0:T(8,128)(2,1)}, bf16[2,2,32,2176]{3,2,1,0:T(8,128)(2,1)}, u32[]{:S(2)}, u32[]{:S(2)}) collective-permute-start(bf16[2,2,32,2176]{3,2,1,0:T(8,128)(2,1)} %pad_maximum_fusion), channel_id=1, source_target_pairs={{0,4},{1,3},{2,6},{3,1},{4,0},{5,7},{6,2},{7,5},{8,12},{9,11},{10,... | collective-permute-start | bytes 1671176 | tf_op jit(solution)/shard_map/ppermute | solution.py:150
  61.8 4.8 %collective-permute-done.14 = bf16[2,2,32,2176]{3,2,1,0:T(8,128)(2,1)} collective-permute-done((bf16[2,2,32,2176]{3,2,1,0:T(8,128)(2,1)}, bf16[2,2,32,2176]{3,2,1,0:T(8,128)(2,1)}, u32[]{:S(2)}, u32[]{:S(2)}) %collective-permute-start.14) | collective-permute-done | bytes 557088 | tf_op jit(solution)/shard_map/ppermute | solution.py:150
  66.6 1.9 %copy-done.2 = bf16[1,2048,768]{2,1,0:T(8,128)(2,1)S(1)} copy-done((bf16[1,2048,768]{2,1,0:T(8,128)(2,1)S(1)}, bf16[1,2048,768]{2,1,0:T(8,128)(2,1)}, u32[]{:S(2)}) %copy-start.2) | copy-done | bytes 3145752
  69.0 1.3 %copy-done = bf16[1,768,2048]{2,1,0:T(8,128)(2,1)S(1)} copy-done((bf16[1,768,2048]{2,1,0:T(8,128)(2,1)S(1)}, bf16[1,768,2048]{2,1,0:T(8,128)(2,1)}, u32[]{:S(2)}) %copy-start) | copy-done | bytes 3145752
  71.0 1.1 touch.3.chip_ref
  72.8 7.2 %experts.3 = (bf16[128,2048]{1,0:T(8,128)(2,1)S(1)}, bf16[128,2048]{1,0:T(8,128)(2,1)S(1)}, bf16[128,2048]{1,0:T(8,128)(2,1)S(1)}, bf16[128,2048]{1,0:T(8,128)(2,1)S(1)}) custom-call(s32[1]{0:T(128)} %touch.3.chip_ref, bf16[1,2048,768]{2,1,0:T(8,128)(2,1)S(1)} %copy-done.1, bf16[1,2048,768]{2,1,0:T(8,128)(2,1)S(1)} %copy-done.3, ...), custom_call_target="tpu_custom_call" | custom-call | flops 9663676416 | bytes 9437184 | tf_op jit(solution)/shard_map/experts/pallas_call | solution.py:111
  80.4 6.8 %experts.2 = (bf16[128,2048]{1,0:T(8,128)(2,1)S(1)}, bf16[128,2048]{1,0:T(8,128)(2,1)S(1)}, bf16[128,2048]{1,0:T(8,128)(2,1)S(1)}, bf16[128,2048]{1,0:T(8,128)(2,1)S(1)}) custom-call(s32[1]{0:T(128)} %touch.3.chip_ref, bf16[1,2048,768]{2,1,0:T(8,128)(2,1)S(1)} %copy-done.1, bf16[1,2048,768]{2,1,0:T(8,128)(2,1)S(1)} %copy-done.3, ...), custom_call_target="tpu_custom_call" | custom-call | flops 9663676416 | bytes 9437184 | tf_op jit(solution)/shard_map/experts/pallas_call | solution.py:111
  88.0 1.6 %collective-permute-start.19 = (bf16[2,2,32,2048]{3,2,1,0:T(8,128)(2,1)S(1)}, bf16[2,2,32,2048]{3,2,1,0:T(8,128)(2,1)S(1)}, u32[]{:S(2)}, u32[]{:S(2)}) collective-permute-start(bf16[2,2,32,2048]{3,2,1,0:T(8,128)(2,1)S(1)} %fusion), channel_id=1, source_target_pairs={{0,4},{1,3},{2,6},{3,1},{4,0},{5,7},{6,2},{7,5},{8,12},{9,11},{10,... | collective-permute-start | bytes 1572872 | tf_op jit(solution)/shard_map/ppermute | solution.py:150
  89.7 1.4 %collective-permute-start.8 = (bf16[2,2,32,2048]{3,2,1,0:T(8,128)(2,1)S(1)}, bf16[2,2,32,2048]{3,2,1,0:T(8,128)(2,1)S(1)}, u32[]{:S(2)}, u32[]{:S(2)}) collective-permute-start(bf16[2,2,32,2048]{3,2,1,0:T(8,128)(2,1)S(1)} %fusion.3), channel_id=1, source_target_pairs={{0,4},{1,3},{2,6},{3,1},{4,0},{5,7},{6,2},{7,5},{8,12},{9,11},{10,... | collective-permute-start | bytes 1572872 | tf_op jit(solution)/shard_map/ppermute | solution.py:150
  91.1 6.1 %collective-permute-done.19 = bf16[2,2,32,2048]{3,2,1,0:T(8,128)(2,1)S(1)} collective-permute-done((bf16[2,2,32,2048]{3,2,1,0:T(8,128)(2,1)S(1)}, bf16[2,2,32,2048]{3,2,1,0:T(8,128)(2,1)S(1)}, u32[]{:S(2)}, u32[]{:S(2)}) %collective-permute-start.19) | collective-permute-done | bytes 524320 | tf_op jit(solution)/shard_map/ppermute | solution.py:150
  97.5 1.6 %collective-permute-start.20 = (bf16[2,32,2048]{2,1,0:T(8,128)(2,1)S(1)}, bf16[2,32,2048]{2,1,0:T(8,128)(2,1)S(1)}, u32[]{:S(2)}, u32[]{:S(2)}) collective-permute-start(bf16[2,32,2048]{2,1,0:T(8,128)(2,1)S(1)} %slice_bitcast_fusion), channel_id=1, source_target_pairs={{0,2},{1,5},{2,0},{3,7},{4,6},{5,1},{6,4},{7,3},{8,10},{9,13},{10,... | collective-permute-start | bytes 786440 | tf_op jit(solution)/shard_map/ppermute | solution.py:150
  99.1 6.6 %collective-permute-done.8 = bf16[2,2,32,2048]{3,2,1,0:T(8,128)(2,1)S(1)} collective-permute-done((bf16[2,2,32,2048]{3,2,1,0:T(8,128)(2,1)S(1)}, bf16[2,2,32,2048]{3,2,1,0:T(8,128)(2,1)S(1)}, u32[]{:S(2)}, u32[]{:S(2)}) %collective-permute-start.8) | collective-permute-done | bytes 524320 | tf_op jit(solution)/shard_map/ppermute | solution.py:150
  105.9 1.6 %collective-permute-start.9 = (bf16[2,32,2048]{2,1,0:T(8,128)(2,1)S(1)}, bf16[2,32,2048]{2,1,0:T(8,128)(2,1)S(1)}, u32[]{:S(2)}, u32[]{:S(2)}) collective-permute-start(bf16[2,32,2048]{2,1,0:T(8,128)(2,1)S(1)} %slice_bitcast_fusion.2), channel_id=1, source_target_pairs={{0,2},{1,5},{2,0},{3,7},{4,6},{5,1},{6,4},{7,3},{8,10},{9,13},{10,... | collective-permute-start | bytes 786440 | tf_op jit(solution)/shard_map/ppermute | solution.py:150
  107.7 1.8 %collective-permute-start.21 = (bf16[32,2048]{1,0:T(8,128)(2,1)S(1)}, bf16[32,2048]{1,0:T(8,128)(2,1)S(1)}, u32[]{:S(2)}, u32[]{:S(2)}) collective-permute-start(bf16[32,2048]{1,0:T(8,128)(2,1)S(1)} %get-tuple-element.32), channel_id=1, source_target_pairs={{0,16},{1,17},{2,18},{3,19},{4,20},{5,21},{6,22},{7,23},{8,24},{9,... | collective-permute-start | bytes 393224 | tf_op jit(solution)/shard_map/ppermute | solution.py:150
  109.5 2.9 %collective-permute-done.9 = bf16[2,32,2048]{2,1,0:T(8,128)(2,1)S(1)} collective-permute-done((bf16[2,32,2048]{2,1,0:T(8,128)(2,1)S(1)}, bf16[2,32,2048]{2,1,0:T(8,128)(2,1)S(1)}, u32[]{:S(2)}, u32[]{:S(2)}) %collective-permute-start.9) | collective-permute-done | bytes 262176 | tf_op jit(solution)/shard_map/ppermute | solution.py:150
  112.5 1.3 %collective-permute-start.10 = (bf16[32,2048]{1,0:T(8,128)(2,1)S(1)}, bf16[32,2048]{1,0:T(8,128)(2,1)S(1)}, u32[]{:S(2)}, u32[]{:S(2)}) collective-permute-start(bf16[32,2048]{1,0:T(8,128)(2,1)S(1)} %slice_bitcast_fusion.6), channel_id=1, source_target_pairs={{0,24},{1,25},{2,26},{3,27},{4,28},{5,29},{6,30},{7,31},{8,0},{9,1... | collective-permute-start | bytes 393224 | tf_op jit(solution)/shard_map/ppermute | solution.py:150
  113.8 1.6 %collective-permute-done.22 = bf16[32,2048]{1,0:T(8,128)(2,1)S(1)} collective-permute-done((bf16[32,2048]{1,0:T(8,128)(2,1)S(1)}, bf16[32,2048]{1,0:T(8,128)(2,1)S(1)}, u32[]{:S(2)}, u32[]{:S(2)}) %collective-permute-start.22) | collective-permute-done | bytes 131104 | tf_op jit(solution)/shard_map/ppermute | solution.py:150
  115.3 2.9 %collective-permute-done.21 = bf16[32,2048]{1,0:T(8,128)(2,1)S(1)} collective-permute-done((bf16[32,2048]{1,0:T(8,128)(2,1)S(1)}, bf16[32,2048]{1,0:T(8,128)(2,1)S(1)}, u32[]{:S(2)}, u32[]{:S(2)}) %collective-permute-start.21) | collective-permute-done | bytes 131104 | tf_op jit(solution)/shard_map/ppermute | solution.py:150
  118.4 1.3 %collective-permute-done.23 = bf16[32,2048]{1,0:T(8,128)(2,1)S(1)} collective-permute-done((bf16[32,2048]{1,0:T(8,128)(2,1)S(1)}, bf16[32,2048]{1,0:T(8,128)(2,1)S(1)}, u32[]{:S(2)}, u32[]{:S(2)}) %collective-permute-start.23) | collective-permute-done | bytes 131104 | tf_op jit(solution)/shard_map/ppermute | solution.py:154
  119.7 0.7 pad_maximum_fusion.4
  (81 shorter events, 8.3 us)
Async XLA Ops:
  0.6 27.0 %copy-start.10 = (s32[64,2]{0,1:T(2,128)S(1)}, s32[64,2]{0,1:T(2,128)}, u32[]{:S(2)}) copy-start(s32[64,2]{0,1:T(2,128)} %param.46) | copy-start | bytes 1540
  0.7 27.6 %copy-start.11 = (f32[64,2]{0,1:T(2,128)S(1)}, f32[64,2]{0,1:T(2,128)}, u32[]{:S(2)}) copy-start(f32[64,2]{0,1:T(2,128)} %param.47) | copy-start | bytes 1540
  0.7 29.9 %copy-start.7 = (bf16[64,2048]{1,0:T(8,128)(2,1)S(1)}, bf16[64,2048]{1,0:T(8,128)(2,1)}, u32[]{:S(2)}) copy-start(bf16[64,2048]{1,0:T(8,128)(2,1)} %hidden_ref.1) | copy-start | bytes 786436
  0.7 31.0 %copy-start.8 = (f32[2048]{0:T(1024)S(1)}, f32[2048]{0:T(1024)}, u32[]{:S(2)}) copy-start(f32[2048]{0:T(1024)} %param.38) | copy-start | bytes 24580
  27.0 39.5 %copy-start.9 = (bf16[2048]{0:T(1024)(128)(2,1)S(1)}, bf16[2048]{0:T(1024)(128)(2,1)}, u32[]{:S(2)}) copy-start(bf16[2048]{0:T(1024)(128)(2,1)} %param.39) | copy-start | bytes 12292
  27.1 39.5 %copy-start.1 = (bf16[1,2048,768]{2,1,0:T(8,128)(2,1)S(1)}, bf16[1,2048,768]{2,1,0:T(8,128)(2,1)}, u32[]{:S(2)}) copy-start(bf16[1,2048,768]{2,1,0:T(8,128)(2,1)} %expert_gate_ref.3) | copy-start | bytes 9437188
  27.1 3.5 %collective-permute-start = (bf16[32,2048]{1,0:T(8,128)(2,1)}, bf16[32,2048]{1,0:T(8,128)(2,1)}, u32[]{:S(2)}, u32[]{:S(2)}) collective-permute-start(bf16[32,2048]{1,0:T(8,128)(2,1)} %get-tuple-element.14), channel_id=1, source_target_pairs={{0,1},{1,0},{2,3},{3,2},{4,5},{5,4},{6,7},{7,6},{8,9},{9,8},{10,11... | collective-permute-start | bytes 393224 | tf_op jit(solution)/shard_map/ppermute | solution.py:154
  31.8 8.8 %collective-permute-start.12 = (bf16[32,2176]{1,0:T(8,128)(2,1)S(1)}, bf16[32,2176]{1,0:T(8,128)(2,1)S(1)}, u32[]{:S(2)}, u32[]{:S(2)}) collective-permute-start(bf16[32,2176]{1,0:T(8,128)(2,1)S(1)} %get-tuple-element.35), channel_id=1, source_target_pairs={{0,24},{1,25},{2,26},{3,27},{4,28},{5,29},{6,30},{7,31},{8,0},{9,1... | collective-permute-start | bytes 417800 | tf_op jit(solution)/shard_map/ppermute | solution.py:150
  36.5 12.7 %collective-permute-start.11 = (bf16[32,2176]{1,0:T(8,128)(2,1)S(1)}, bf16[32,2176]{1,0:T(8,128)(2,1)S(1)}, u32[]{:S(2)}, u32[]{:S(2)}) collective-permute-start(bf16[32,2176]{1,0:T(8,128)(2,1)S(1)} %get-tuple-element.35), channel_id=1, source_target_pairs={{0,16},{1,17},{2,18},{3,19},{4,20},{5,21},{6,22},{7,23},{8,24},{9,... | collective-permute-start | bytes 417800 | tf_op jit(solution)/shard_map/ppermute | solution.py:150
  36.5 14.3 %collective-permute-start.1 = (bf16[32,2176]{1,0:T(8,128)(2,1)S(1)}, bf16[32,2176]{1,0:T(8,128)(2,1)S(1)}, u32[]{:S(2)}, u32[]{:S(2)}) collective-permute-start(bf16[32,2176]{1,0:T(8,128)(2,1)S(1)} %get-tuple-element.35), channel_id=1, source_target_pairs={{0,8},{1,9},{2,10},{3,11},{4,12},{5,13},{6,14},{7,15},{8,16},{9,17... | collective-permute-start | bytes 417800 | tf_op jit(solution)/shard_map/ppermute | solution.py:150
  49.2 6.6 %collective-permute-start.13 = (bf16[2,32,2176]{2,1,0:T(8,128)(2,1)S(1)}, bf16[2,32,2176]{2,1,0:T(8,128)(2,1)S(1)}, u32[]{:S(2)}, u32[]{:S(2)}) collective-permute-start(bf16[2,32,2176]{2,1,0:T(8,128)(2,1)S(1)} %get-tuple-element.29), channel_id=1, source_target_pairs={{0,2},{1,5},{2,0},{3,7},{4,6},{5,1},{6,4},{7,3},{8,10},{9,13},{10,... | collective-permute-start | bytes 835592 | tf_op jit(solution)/shard_map/ppermute | solution.py:150
  50.8 8.6 %collective-permute-start.2 = (bf16[2,32,2176]{2,1,0:T(8,128)(2,1)S(1)}, bf16[2,32,2176]{2,1,0:T(8,128)(2,1)S(1)}, u32[]{:S(2)}, u32[]{:S(2)}) collective-permute-start(bf16[2,32,2176]{2,1,0:T(8,128)(2,1)S(1)} %get-tuple-element.27), channel_id=1, source_target_pairs={{0,2},{1,5},{2,0},{3,7},{4,6},{5,1},{6,4},{7,3},{8,10},{9,13},{10,... | collective-permute-start | bytes 835592 | tf_op jit(solution)/shard_map/ppermute | solution.py:150
  56.7 9.8 %collective-permute-start.14 = (bf16[2,2,32,2176]{3,2,1,0:T(8,128)(2,1)}, bf16[2,2,32,2176]{3,2,1,0:T(8,128)(2,1)}, u32[]{:S(2)}, u32[]{:S(2)}) collective-permute-start(bf16[2,2,32,2176]{3,2,1,0:T(8,128)(2,1)} %pad_maximum_fusion.1), channel_id=1, source_target_pairs={{0,4},{1,3},{2,6},{3,1},{4,0},{5,7},{6,2},{7,5},{8,12},{9,11},{10,... | collective-permute-start | bytes 1671176 | tf_op jit(solution)/shard_map/ppermute | solution.py:150
  60.2 12.4 %collective-permute-start.3 = (bf16[2,2,32,2176]{3,2,1,0:T(8,128)(2,1)}, bf16[2,2,32,2176]{3,2,1,0:T(8,128)(2,1)}, u32[]{:S(2)}, u32[]{:S(2)}) collective-permute-start(bf16[2,2,32,2176]{3,2,1,0:T(8,128)(2,1)} %pad_maximum_fusion), channel_id=1, source_target_pairs={{0,4},{1,3},{2,6},{3,1},{4,0},{5,7},{6,2},{7,5},{8,12},{9,11},{10,... | collective-permute-start | bytes 1671176 | tf_op jit(solution)/shard_map/ppermute | solution.py:150
  61.8 11.0 %collective-permute-start.15 = (bf16[2,2,32,2176]{3,2,1,0:T(8,128)(2,1)}, bf16[2,2,32,2176]{3,2,1,0:T(8,128)(2,1)}, u32[]{:S(2)}, u32[]{:S(2)}) collective-permute-start(bf16[2,2,32,2176]{3,2,1,0:T(8,128)(2,1)} %pad_maximum_fusion.1), channel_id=1, source_target_pairs={{0,1},{1,0},{2,3},{3,2},{4,5},{5,4},{6,7},{7,6},{8,9},{9,8},{10,11... | collective-permute-start | bytes 1671176 | tf_op jit(solution)/shard_map/ppermute | solution.py:154
  66.5 6.2 %collective-permute-start.16 = (bf16[2,2,32,2176]{3,2,1,0:T(8,128)(2,1)}, bf16[2,2,32,2176]{3,2,1,0:T(8,128)(2,1)}, u32[]{:S(2)}, u32[]{:S(2)}) collective-permute-start(bf16[2,2,32,2176]{3,2,1,0:T(8,128)(2,1)} %collective-permute-done.14), channel_id=1, source_target_pairs={{0,1},{1,0},{2,3},{3,2},{4,5},{5,4},{6,7},{7,6},{8,9},{9,8},{10,11... | collective-permute-start | bytes 1671176 | tf_op jit(solution)/shard_map/ppermute | solution.py:154
  68.4 2.5 %copy-start.6 = (bf16[176,2048]{1,0:T(8,128)(2,1)S(1)}, bf16[176,2048]{1,0:T(8,128)(2,1)}, u32[]{:S(2)}) copy-start(bf16[176,2048]{1,0:T(8,128)(2,1)} %dense_down_ref.3) | copy-start | bytes 2162692
  69.0 3.8 %copy-start.3 = (bf16[1,2048,768]{2,1,0:T(8,128)(2,1)S(1)}, bf16[1,2048,768]{2,1,0:T(8,128)(2,1)}, u32[]{:S(2)}) copy-start(bf16[1,2048,768]{2,1,0:T(8,128)(2,1)} %expert_up_ref.3) | copy-start | bytes 9437188
  72.1 8.3 %collective-permute-start.4 = (bf16[2,2,32,2176]{3,2,1,0:T(8,128)(2,1)}, bf16[2,2,32,2176]{3,2,1,0:T(8,128)(2,1)S(1)}, u32[]{:S(2)}, u32[]{:S(2)}) collective-permute-start(bf16[2,2,32,2176]{3,2,1,0:T(8,128)(2,1)} %pad_maximum_fusion), channel_id=1, source_target_pairs={{0,1},{1,0},{2,3},{3,2},{4,5},{5,4},{6,7},{7,6},{8,9},{9,8},{10,11... | collective-permute-start | bytes 1671176 | tf_op jit(solution)/shard_map/ppermute | solution.py:154
  72.7 7.8 %collective-permute-start.5 = (bf16[2,2,32,2176]{3,2,1,0:T(8,128)(2,1)}, bf16[2,2,32,2176]{3,2,1,0:T(8,128)(2,1)S(1)}, u32[]{:S(2)}, u32[]{:S(2)}) collective-permute-start(bf16[2,2,32,2176]{3,2,1,0:T(8,128)(2,1)} %collective-permute-done.3), channel_id=1, source_target_pairs={{0,1},{1,0},{2,3},{3,2},{4,5},{5,4},{6,7},{7,6},{8,9},{9,8},{10,11... | collective-permute-start | bytes 1671176 | tf_op jit(solution)/shard_map/ppermute | solution.py:154
  79.9 7.9 %collective-permute-start.18 = (bf16[2,2,32,2048]{3,2,1,0:T(8,128)(2,1)S(1)}, bf16[2,2,32,2048]{3,2,1,0:T(8,128)(2,1)S(1)}, u32[]{:S(2)}, u32[]{:S(2)}) collective-permute-start(bf16[2,2,32,2048]{3,2,1,0:T(8,128)(2,1)S(1)} %bitcast.87), channel_id=1, source_target_pairs={{0,1},{1,0},{2,3},{3,2},{4,5},{5,4},{6,7},{7,6},{8,9},{9,8},{10,11... | collective-permute-start | bytes 1572872 | tf_op jit(solution)/shard_map/ppermute | solution.py:154
  87.3 2.3 %collective-permute-start.7 = (bf16[2,2,32,2048]{3,2,1,0:T(8,128)(2,1)S(1)}, bf16[2,2,32,2048]{3,2,1,0:T(8,128)(2,1)S(1)}, u32[]{:S(2)}, u32[]{:S(2)}) collective-permute-start(bf16[2,2,32,2048]{3,2,1,0:T(8,128)(2,1)S(1)} %bitcast.88), channel_id=1, source_target_pairs={{0,1},{1,0},{2,3},{3,2},{4,5},{5,4},{6,7},{7,6},{8,9},{9,8},{10,11... | collective-permute-start | bytes 1572872 | tf_op jit(solution)/shard_map/ppermute | solution.py:154
  87.4 3.7 %collective-permute-start.17 = (bf16[2,2,32,2048]{3,2,1,0:T(8,128)(2,1)S(1)}, bf16[2,2,32,2048]{3,2,1,0:T(8,128)(2,1)S(1)}, u32[]{:S(2)}, u32[]{:S(2)}) collective-permute-start(bf16[2,2,32,2048]{3,2,1,0:T(8,128)(2,1)S(1)} %bitcast.85), channel_id=1, source_target_pairs={{0,1},{1,0},{2,3},{3,2},{4,5},{5,4},{6,7},{7,6},{8,9},{9,8},{10,11... | collective-permute-start | bytes 1572872 | tf_op jit(solution)/shard_map/ppermute | solution.py:154
  88.0 9.2 %collective-permute-start.19 = (bf16[2,2,32,2048]{3,2,1,0:T(8,128)(2,1)S(1)}, bf16[2,2,32,2048]{3,2,1,0:T(8,128)(2,1)S(1)}, u32[]{:S(2)}, u32[]{:S(2)}) collective-permute-start(bf16[2,2,32,2048]{3,2,1,0:T(8,128)(2,1)S(1)} %fusion), channel_id=1, source_target_pairs={{0,4},{1,3},{2,6},{3,1},{4,0},{5,7},{6,2},{7,5},{8,12},{9,11},{10,... | collective-permute-start | bytes 1572872 | tf_op jit(solution)/shard_map/ppermute | solution.py:150
  89.6 9.5 %collective-permute-start.6 = (bf16[2,2,32,2048]{3,2,1,0:T(8,128)(2,1)S(1)}, bf16[2,2,32,2048]{3,2,1,0:T(8,128)(2,1)S(1)}, u32[]{:S(2)}, u32[]{:S(2)}) collective-permute-start(bf16[2,2,32,2048]{3,2,1,0:T(8,128)(2,1)S(1)} %bitcast.86), channel_id=1, source_target_pairs={{0,1},{1,0},{2,3},{3,2},{4,5},{5,4},{6,7},{7,6},{8,9},{9,8},{10,11... | collective-permute-start | bytes 1572872 | tf_op jit(solution)/shard_map/ppermute | solution.py:154
  89.7 15.9 %collective-permute-start.8 = (bf16[2,2,32,2048]{3,2,1,0:T(8,128)(2,1)S(1)}, bf16[2,2,32,2048]{3,2,1,0:T(8,128)(2,1)S(1)}, u32[]{:S(2)}, u32[]{:S(2)}) collective-permute-start(bf16[2,2,32,2048]{3,2,1,0:T(8,128)(2,1)S(1)} %fusion.3), channel_id=1, source_target_pairs={{0,4},{1,3},{2,6},{3,1},{4,0},{5,7},{6,2},{7,5},{8,12},{9,11},{10,... | collective-permute-start | bytes 1572872 | tf_op jit(solution)/shard_map/ppermute | solution.py:150
  97.5 10.0 %collective-permute-start.20 = (bf16[2,32,2048]{2,1,0:T(8,128)(2,1)S(1)}, bf16[2,32,2048]{2,1,0:T(8,128)(2,1)S(1)}, u32[]{:S(2)}, u32[]{:S(2)}) collective-permute-start(bf16[2,32,2048]{2,1,0:T(8,128)(2,1)S(1)} %slice_bitcast_fusion), channel_id=1, source_target_pairs={{0,2},{1,5},{2,0},{3,7},{4,6},{5,1},{6,4},{7,3},{8,10},{9,13},{10,... | collective-permute-start | bytes 786440 | tf_op jit(solution)/shard_map/ppermute | solution.py:150
  105.9 6.4 %collective-permute-start.9 = (bf16[2,32,2048]{2,1,0:T(8,128)(2,1)S(1)}, bf16[2,32,2048]{2,1,0:T(8,128)(2,1)S(1)}, u32[]{:S(2)}, u32[]{:S(2)}) collective-permute-start(bf16[2,32,2048]{2,1,0:T(8,128)(2,1)S(1)} %slice_bitcast_fusion.2), channel_id=1, source_target_pairs={{0,2},{1,5},{2,0},{3,7},{4,6},{5,1},{6,4},{7,3},{8,10},{9,13},{10,... | collective-permute-start | bytes 786440 | tf_op jit(solution)/shard_map/ppermute | solution.py:150
  107.6 7.7 %collective-permute-start.22 = (bf16[32,2048]{1,0:T(8,128)(2,1)S(1)}, bf16[32,2048]{1,0:T(8,128)(2,1)S(1)}, u32[]{:S(2)}, u32[]{:S(2)}) collective-permute-start(bf16[32,2048]{1,0:T(8,128)(2,1)S(1)} %get-tuple-element.33), channel_id=1, source_target_pairs={{0,8},{1,9},{2,10},{3,11},{4,12},{5,13},{6,14},{7,15},{8,16},{9,17... | collective-permute-start | bytes 393224 | tf_op jit(solution)/shard_map/ppermute | solution.py:150
  107.7 10.5 %collective-permute-start.21 = (bf16[32,2048]{1,0:T(8,128)(2,1)S(1)}, bf16[32,2048]{1,0:T(8,128)(2,1)S(1)}, u32[]{:S(2)}, u32[]{:S(2)}) collective-permute-start(bf16[32,2048]{1,0:T(8,128)(2,1)S(1)} %get-tuple-element.32), channel_id=1, source_target_pairs={{0,16},{1,17},{2,18},{3,19},{4,20},{5,21},{6,22},{7,23},{8,24},{9,... | collective-permute-start | bytes 393224 | tf_op jit(solution)/shard_map/ppermute | solution.py:150
  112.5 5.8 %collective-permute-start.10 = (bf16[32,2048]{1,0:T(8,128)(2,1)S(1)}, bf16[32,2048]{1,0:T(8,128)(2,1)S(1)}, u32[]{:S(2)}, u32[]{:S(2)}) collective-permute-start(bf16[32,2048]{1,0:T(8,128)(2,1)S(1)} %slice_bitcast_fusion.6), channel_id=1, source_target_pairs={{0,24},{1,25},{2,26},{3,27},{4,28},{5,29},{6,30},{7,31},{8,0},{9,1... | collective-permute-start | bytes 393224 | tf_op jit(solution)/shard_map/ppermute | solution.py:150
  118.3 1.4 %collective-permute-start.23 = (bf16[32,2048]{1,0:T(8,128)(2,1)S(1)}, bf16[32,2048]{1,0:T(8,128)(2,1)S(1)}, u32[]{:S(2)}, u32[]{:S(2)}) collective-permute-start(bf16[32,2048]{1,0:T(8,128)(2,1)S(1)} %fusion.14), channel_id=1, source_target_pairs={{0,1},{1,0},{2,3},{3,2},{4,5},{5,4},{6,7},{7,6},{8,9},{9,8},{10,11... | collective-permute-start | bytes 393224 | tf_op jit(solution)/shard_map/ppermute | solution.py:154
  (4 other events, 8.1 us)

commit v2 on v1

--- a/solution.py
+++ b/solution.py
@@ -243,28 +243,30 @@
     ones = jnp.ones((size, 128), jnp.bfloat16)
     lane = lax.broadcasted_iota(jnp.int32, (size, 128), 1)
 
+    own = lax.broadcasted_iota(jnp.int32, (size, 2 * block), 1) % block
+    blank = jnp.zeros((block, size), jnp.float32)
+
     def pulled(head):
-        unit = unit_scr[head, rows, :]
-        products = [
-            (state_ref[seq, head] * unit[seq : seq + 1]).astype(jnp.bfloat16)
+        unit = jnp.concatenate([unit_scr[head, rows, :], blank]).astype(jnp.bfloat16)
+        states = [state_ref[seq, head].astype(jnp.bfloat16) for seq in range(block)]
+        return flat_dot(jnp.concatenate(states), unit)
+
+    def updated(head, removed):
+        decay = decay_scr[head, rows, :]
+        recept = recept_scr[head, rows, :]
+        upright = jnp.concatenate([blank, value_scr[head, rows, :]]).T
+        factors = [
+            jnp.where(own == seq, removed[seq * size : (seq + 1) * size] + upright, 0.0)
             for seq in range(block)
         ]
-        return matmul(jnp.concatenate(products), ones)
-
-    def updated(head, removed):
-        pull = pull_scr[head, rows, :]
-        push = push_scr[head, rows, :]
-        decay = decay_scr[head, rows, :]
-        recept = recept_scr[head, rows, :]
-        value = value_scr[head, rows, :].T
+        changes = jnp.concatenate([-pull_scr[head, rows, :], push_scr[head, rows, :]])
+        change = matmul(
+            jnp.concatenate(factors).astype(jnp.bfloat16), changes.astype(jnp.bfloat16)
+        )
         products = []
         for seq in range(block):
             one = slice(seq, seq + 1)
-            fresh = (
-                state_ref[seq, head] * decay[one]
-                - removed[seq * size : (seq + 1) * size, :size] * pull[one]
-                + value[:, one] * push[one]
-            )
+            fresh = state_ref[seq, head] * decay[one] + change[seq * size : (seq + 1) * size]
             new_ref[seq, head] = fresh
             products.append((fresh * recept[one]).astype(jnp.bfloat16))
         return matmul(jnp.concatenate(products), ones)

time: 121 us -> 120 us (level)
  no operation moved by 1% of the time
where the time goes in v2:
time: 120 us
  waiting for transfers between devices  43.5 us (36%)
  Pallas kernels  41.4 us (34%)
  starting transfers between devices  22.4 us (19%)
  other arithmetic  7.03 us (6%)
  local copies, waits for them, and re-layouts  4.53 us (4%)
    ppermute x14, waiting for transfers between devices, hop(): return lax.ppermute(value, ('ep', 'tp'), perm)  42.1 us
    pallas_call x1, Pallas kernels, attention(): pl.pallas_call(attention_kernel, grid_spec=pltpu.PrefetchScalarGridSpec(n...  25.8 us
    ppermute x14, starting transfers between devices, hop(): return lax.ppermute(value, ('ep', 'tp'), perm)  20.1 us
    pallas_call x2, Pallas kernels, experts(): pl.pallas_call(functools.partial(experts_kernel, tuple(pieces), cap, span...  14 us
    unnamed x25, local copies, waits for them, and re-layouts  3.97 us
  transfers between devices with their start and end apart: 24, of which 11 were waited for; matrix products, arithmetic and copies ran while one was open for 5% of the time, Pallas kernels for 13%

profile of v2, /device:TPU:0, one launch (start us, length us, event | category | flops | bytes accessed | tf_op | source)
XLA Modules:
  0.0 119.9 jit_solution(18060552130907018918)
XLA Ops:
  0.7 25.8 %attention.1 = (bf16[32,2048]{1,0:T(8,128)(2,1)}, bf16[32,2048]{1,0:T(8,128)(2,1)}, f32[64,8,64,64]{3,2,1,0:T(8,128)}) custom-call(s32[1]{0:T(128)} %bitcast.core_ref, bf16[64,2048]{1,0:T(8,128)(2,1)} %hidden_ref.1, f32[1,2048]{1,0:T(1,128)} %bitcast.96, bf16[2048,512]{1,0:T(8,128)(2,1)} %recept_ref.1, bf16[2048,512]{1,0:T(8,128)(2,1)} %key_ref.1, ...), custom_call_target="tpu_custom_call" | custom-call | tf_op jit(solution)/shard_map/attention/pallas_call | solution.py:332
  30.0 1.1 fusion.8
  31.3 4.7 %collective-permute-start.12 = (bf16[32,2176]{1,0:T(8,128)(2,1)S(1)}, bf16[32,2176]{1,0:T(8,128)(2,1)S(1)}, u32[]{:S(2)}, u32[]{:S(2)}) collective-permute-start(bf16[32,2176]{1,0:T(8,128)(2,1)S(1)} %get-tuple-element.35), channel_id=1, source_target_pairs={{0,24},{1,25},{2,26},{3,27},{4,28},{5,29},{6,30},{7,31},{8,0},{9,1... | collective-permute-start | bytes 417800 | tf_op jit(solution)/shard_map/ppermute | solution.py:150
  35.9 1.0 collective-permute-start.1
  36.9 3.1 %collective-permute-done.12 = bf16[32,2176]{1,0:T(8,128)(2,1)S(1)} collective-permute-done((bf16[32,2176]{1,0:T(8,128)(2,1)S(1)}, bf16[32,2176]{1,0:T(8,128)(2,1)S(1)}, u32[]{:S(2)}, u32[]{:S(2)}) %collective-permute-start.12) | collective-permute-done | bytes 139296 | tf_op jit(solution)/shard_map/ppermute | solution.py:150
  40.1 8.5 %collective-permute-done.11 = bf16[32,2176]{1,0:T(8,128)(2,1)S(1)} collective-permute-done((bf16[32,2176]{1,0:T(8,128)(2,1)S(1)}, bf16[32,2176]{1,0:T(8,128)(2,1)S(1)}, u32[]{:S(2)}, u32[]{:S(2)}) %collective-permute-start.11) | collective-permute-done | bytes 139296 | tf_op jit(solution)/shard_map/ppermute | solution.py:150
  48.6 1.6 %collective-permute-start.13 = (bf16[2,32,2176]{2,1,0:T(8,128)(2,1)S(1)}, bf16[2,32,2176]{2,1,0:T(8,128)(2,1)S(1)}, u32[]{:S(2)}, u32[]{:S(2)}) collective-permute-start(bf16[2,32,2176]{2,1,0:T(8,128)(2,1)S(1)} %get-tuple-element.29), channel_id=1, source_target_pairs={{0,2},{1,5},{2,0},{3,7},{4,6},{5,1},{6,4},{7,3},{8,10},{9,13},{10,... | collective-permute-start | bytes 835592 | tf_op jit(solution)/shard_map/ppermute | solution.py:150
  50.8 4.4 %collective-permute-done.13 = bf16[2,32,2176]{2,1,0:T(8,128)(2,1)S(1)} collective-permute-done((bf16[2,32,2176]{2,1,0:T(8,128)(2,1)S(1)}, bf16[2,32,2176]{2,1,0:T(8,128)(2,1)S(1)}, u32[]{:S(2)}, u32[]{:S(2)}) %collective-permute-start.13) | collective-permute-done | bytes 278560 | tf_op jit(solution)/shard_map/ppermute | solution.py:150
  55.2 0.9 pad_maximum_fusion.1
  56.1 1.5 %collective-permute-start.14 = (bf16[2,2,32,2176]{3,2,1,0:T(8,128)(2,1)}, bf16[2,2,32,2176]{3,2,1,0:T(8,128)(2,1)}, u32[]{:S(2)}, u32[]{:S(2)}) collective-permute-start(bf16[2,2,32,2176]{3,2,1,0:T(8,128)(2,1)} %pad_maximum_fusion.1), channel_id=1, source_target_pairs={{0,4},{1,3},{2,6},{3,1},{4,0},{5,7},{6,2},{7,5},{8,12},{9,11},{10,... | collective-permute-start | bytes 1671176 | tf_op jit(solution)/shard_map/ppermute | solution.py:150
  57.6 1.2 collective-permute-done.2
  58.8 0.9 pad_maximum_fusion
  59.7 1.5 %collective-permute-start.3 = (bf16[2,2,32,2176]{3,2,1,0:T(8,128)(2,1)}, bf16[2,2,32,2176]{3,2,1,0:T(8,128)(2,1)}, u32[]{:S(2)}, u32[]{:S(2)}) collective-permute-start(bf16[2,2,32,2176]{3,2,1,0:T(8,128)(2,1)} %pad_maximum_fusion), channel_id=1, source_target_pairs={{0,4},{1,3},{2,6},{3,1},{4,0},{5,7},{6,2},{7,5},{8,12},{9,11},{10,... | collective-permute-start | bytes 1671176 | tf_op jit(solution)/shard_map/ppermute | solution.py:150
  61.2 4.7 %collective-permute-done.14 = bf16[2,2,32,2176]{3,2,1,0:T(8,128)(2,1)} collective-permute-done((bf16[2,2,32,2176]{3,2,1,0:T(8,128)(2,1)}, bf16[2,2,32,2176]{3,2,1,0:T(8,128)(2,1)}, u32[]{:S(2)}, u32[]{:S(2)}) %collective-permute-start.14) | collective-permute-done | bytes 557088 | tf_op jit(solution)/shard_map/ppermute | solution.py:150
  66.0 1.9 %copy-done.2 = bf16[1,2048,768]{2,1,0:T(8,128)(2,1)S(1)} copy-done((bf16[1,2048,768]{2,1,0:T(8,128)(2,1)S(1)}, bf16[1,2048,768]{2,1,0:T(8,128)(2,1)}, u32[]{:S(2)}) %copy-start.2) | copy-done | bytes 3145752
  68.4 1.3 %copy-done = bf16[1,768,2048]{2,1,0:T(8,128)(2,1)S(1)} copy-done((bf16[1,768,2048]{2,1,0:T(8,128)(2,1)S(1)}, bf16[1,768,2048]{2,1,0:T(8,128)(2,1)}, u32[]{:S(2)}) %copy-start) | copy-done | bytes 3145752
  70.4 1.1 touch.3.chip_ref
  72.2 7.2 %experts.3 = (bf16[128,2048]{1,0:T(8,128)(2,1)S(1)}, bf16[128,2048]{1,0:T(8,128)(2,1)S(1)}, bf16[128,2048]{1,0:T(8,128)(2,1)S(1)}, bf16[128,2048]{1,0:T(8,128)(2,1)S(1)}) custom-call(s32[1]{0:T(128)} %touch.3.chip_ref, bf16[1,2048,768]{2,1,0:T(8,128)(2,1)S(1)} %copy-done.1, bf16[1,2048,768]{2,1,0:T(8,128)(2,1)S(1)} %copy-done.3, ...), custom_call_target="tpu_custom_call" | custom-call | flops 9663676416 | bytes 9437184 | tf_op jit(solution)/shard_map/experts/pallas_call | solution.py:111
  79.9 6.8 %experts.2 = (bf16[128,2048]{1,0:T(8,128)(2,1)S(1)}, bf16[128,2048]{1,0:T(8,128)(2,1)S(1)}, bf16[128,2048]{1,0:T(8,128)(2,1)S(1)}, bf16[128,2048]{1,0:T(8,128)(2,1)S(1)}) custom-call(s32[1]{0:T(128)} %touch.3.chip_ref, bf16[1,2048,768]{2,1,0:T(8,128)(2,1)S(1)} %copy-done.1, bf16[1,2048,768]{2,1,0:T(8,128)(2,1)S(1)} %copy-done.3, ...), custom_call_target="tpu_custom_call" | custom-call | flops 9663676416 | bytes 9437184 | tf_op jit(solution)/shard_map/experts/pallas_call | solution.py:111
  87.4 1.6 %collective-permute-start.19 = (bf16[2,2,32,2048]{3,2,1,0:T(8,128)(2,1)S(1)}, bf16[2,2,32,2048]{3,2,1,0:T(8,128)(2,1)S(1)}, u32[]{:S(2)}, u32[]{:S(2)}) collective-permute-start(bf16[2,2,32,2048]{3,2,1,0:T(8,128)(2,1)S(1)} %fusion), channel_id=1, source_target_pairs={{0,4},{1,3},{2,6},{3,1},{4,0},{5,7},{6,2},{7,5},{8,12},{9,11},{10,... | collective-permute-start | bytes 1572872 | tf_op jit(solution)/shard_map/ppermute | solution.py:150
  89.1 1.4 %collective-permute-start.8 = (bf16[2,2,32,2048]{3,2,1,0:T(8,128)(2,1)S(1)}, bf16[2,2,32,2048]{3,2,1,0:T(8,128)(2,1)S(1)}, u32[]{:S(2)}, u32[]{:S(2)}) collective-permute-start(bf16[2,2,32,2048]{3,2,1,0:T(8,128)(2,1)S(1)} %fusion.3), channel_id=1, source_target_pairs={{0,4},{1,3},{2,6},{3,1},{4,0},{5,7},{6,2},{7,5},{8,12},{9,11},{10,... | collective-permute-start | bytes 1572872 | tf_op jit(solution)/shard_map/ppermute | solution.py:150
  90.5 6.2 %collective-permute-done.19 = bf16[2,2,32,2048]{3,2,1,0:T(8,128)(2,1)S(1)} collective-permute-done((bf16[2,2,32,2048]{3,2,1,0:T(8,128)(2,1)S(1)}, bf16[2,2,32,2048]{3,2,1,0:T(8,128)(2,1)S(1)}, u32[]{:S(2)}, u32[]{:S(2)}) %collective-permute-start.19) | collective-permute-done | bytes 524320 | tf_op jit(solution)/shard_map/ppermute | solution.py:150
  96.9 1.6 %collective-permute-start.20 = (bf16[2,32,2048]{2,1,0:T(8,128)(2,1)S(1)}, bf16[2,32,2048]{2,1,0:T(8,128)(2,1)S(1)}, u32[]{:S(2)}, u32[]{:S(2)}) collective-permute-start(bf16[2,32,2048]{2,1,0:T(8,128)(2,1)S(1)} %slice_bitcast_fusion), channel_id=1, source_target_pairs={{0,2},{1,5},{2,0},{3,7},{4,6},{5,1},{6,4},{7,3},{8,10},{9,13},{10,... | collective-permute-start | bytes 786440 | tf_op jit(solution)/shard_map/ppermute | solution.py:150
  98.5 6.6 %collective-permute-done.8 = bf16[2,2,32,2048]{3,2,1,0:T(8,128)(2,1)S(1)} collective-permute-done((bf16[2,2,32,2048]{3,2,1,0:T(8,128)(2,1)S(1)}, bf16[2,2,32,2048]{3,2,1,0:T(8,128)(2,1)S(1)}, u32[]{:S(2)}, u32[]{:S(2)}) %collective-permute-start.8) | collective-permute-done | bytes 524320 | tf_op jit(solution)/shard_map/ppermute | solution.py:150
  105.4 1.6 %collective-permute-start.9 = (bf16[2,32,2048]{2,1,0:T(8,128)(2,1)S(1)}, bf16[2,32,2048]{2,1,0:T(8,128)(2,1)S(1)}, u32[]{:S(2)}, u32[]{:S(2)}) collective-permute-start(bf16[2,32,2048]{2,1,0:T(8,128)(2,1)S(1)} %slice_bitcast_fusion.2), channel_id=1, source_target_pairs={{0,2},{1,5},{2,0},{3,7},{4,6},{5,1},{6,4},{7,3},{8,10},{9,13},{10,... | collective-permute-start | bytes 786440 | tf_op jit(solution)/shard_map/ppermute | solution.py:150
  107.1 1.8 %collective-permute-start.21 = (bf16[32,2048]{1,0:T(8,128)(2,1)S(1)}, bf16[32,2048]{1,0:T(8,128)(2,1)S(1)}, u32[]{:S(2)}, u32[]{:S(2)}) collective-permute-start(bf16[32,2048]{1,0:T(8,128)(2,1)S(1)} %get-tuple-element.32), channel_id=1, source_target_pairs={{0,16},{1,17},{2,18},{3,19},{4,20},{5,21},{6,22},{7,23},{8,24},{9,... | collective-permute-start | bytes 393224 | tf_op jit(solution)/shard_map/ppermute | solution.py:150
  108.9 2.9 %collective-permute-done.9 = bf16[2,32,2048]{2,1,0:T(8,128)(2,1)S(1)} collective-permute-done((bf16[2,32,2048]{2,1,0:T(8,128)(2,1)S(1)}, bf16[2,32,2048]{2,1,0:T(8,128)(2,1)S(1)}, u32[]{:S(2)}, u32[]{:S(2)}) %collective-permute-start.9) | collective-permute-done | bytes 262176 | tf_op jit(solution)/shard_map/ppermute | solution.py:150
  111.9 1.3 %collective-permute-start.10 = (bf16[32,2048]{1,0:T(8,128)(2,1)S(1)}, bf16[32,2048]{1,0:T(8,128)(2,1)S(1)}, u32[]{:S(2)}, u32[]{:S(2)}) collective-permute-start(bf16[32,2048]{1,0:T(8,128)(2,1)S(1)} %slice_bitcast_fusion.6), channel_id=1, source_target_pairs={{0,24},{1,25},{2,26},{3,27},{4,28},{5,29},{6,30},{7,31},{8,0},{9,1... | collective-permute-start | bytes 393224 | tf_op jit(solution)/shard_map/ppermute | solution.py:150
  113.2 1.6 %collective-permute-done.22 = bf16[32,2048]{1,0:T(8,128)(2,1)S(1)} collective-permute-done((bf16[32,2048]{1,0:T(8,128)(2,1)S(1)}, bf16[32,2048]{1,0:T(8,128)(2,1)S(1)}, u32[]{:S(2)}, u32[]{:S(2)}) %collective-permute-start.22) | collective-permute-done | bytes 131104 | tf_op jit(solution)/shard_map/ppermute | solution.py:150
  114.8 2.9 %collective-permute-done.21 = bf16[32,2048]{1,0:T(8,128)(2,1)S(1)} collective-permute-done((bf16[32,2048]{1,0:T(8,128)(2,1)S(1)}, bf16[32,2048]{1,0:T(8,128)(2,1)S(1)}, u32[]{:S(2)}, u32[]{:S(2)}) %collective-permute-start.21) | collective-permute-done | bytes 131104 | tf_op jit(solution)/shard_map/ppermute | solution.py:150
  117.8 1.3 %collective-permute-done.23 = bf16[32,2048]{1,0:T(8,128)(2,1)S(1)} collective-permute-done((bf16[32,2048]{1,0:T(8,128)(2,1)S(1)}, bf16[32,2048]{1,0:T(8,128)(2,1)S(1)}, u32[]{:S(2)}, u32[]{:S(2)}) %collective-permute-start.23) | collective-permute-done | bytes 131104 | tf_op jit(solution)/shard_map/ppermute | solution.py:154
  119.2 0.7 pad_maximum_fusion.4
  (81 shorter events, 8.3 us)
Async XLA Ops:
  0.6 26.4 %copy-start.10 = (s32[64,2]{0,1:T(2,128)S(1)}, s32[64,2]{0,1:T(2,128)}, u32[]{:S(2)}) copy-start(s32[64,2]{0,1:T(2,128)} %param.46) | copy-start | bytes 1540
  0.7 27.0 %copy-start.11 = (f32[64,2]{0,1:T(2,128)S(1)}, f32[64,2]{0,1:T(2,128)}, u32[]{:S(2)}) copy-start(f32[64,2]{0,1:T(2,128)} %param.47) | copy-start | bytes 1540
  0.7 29.3 %copy-start.7 = (bf16[64,2048]{1,0:T(8,128)(2,1)S(1)}, bf16[64,2048]{1,0:T(8,128)(2,1)}, u32[]{:S(2)}) copy-start(bf16[64,2048]{1,0:T(8,128)(2,1)} %hidden_ref.1) | copy-start | bytes 786436
  0.7 30.4 %copy-start.8 = (f32[2048]{0:T(1024)S(1)}, f32[2048]{0:T(1024)}, u32[]{:S(2)}) copy-start(f32[2048]{0:T(1024)} %param.38) | copy-start | bytes 24580
  26.5 39.5 %copy-start.9 = (bf16[2048]{0:T(1024)(128)(2,1)S(1)}, bf16[2048]{0:T(1024)(128)(2,1)}, u32[]{:S(2)}) copy-start(bf16[2048]{0:T(1024)(128)(2,1)} %param.39) | copy-start | bytes 12292
  26.5 39.5 %copy-start.1 = (bf16[1,2048,768]{2,1,0:T(8,128)(2,1)S(1)}, bf16[1,2048,768]{2,1,0:T(8,128)(2,1)}, u32[]{:S(2)}) copy-start(bf16[1,2048,768]{2,1,0:T(8,128)(2,1)} %expert_gate_ref.3) | copy-start | bytes 9437188
  26.5 3.5 %collective-permute-start = (bf16[32,2048]{1,0:T(8,128)(2,1)}, bf16[32,2048]{1,0:T(8,128)(2,1)}, u32[]{:S(2)}, u32[]{:S(2)}) collective-permute-start(bf16[32,2048]{1,0:T(8,128)(2,1)} %get-tuple-element.14), channel_id=1, source_target_pairs={{0,1},{1,0},{2,3},{3,2},{4,5},{5,4},{6,7},{7,6},{8,9},{9,8},{10,11... | collective-permute-start | bytes 393224 | tf_op jit(solution)/shard_map/ppermute | solution.py:154
  31.3 8.8 %collective-permute-start.12 = (bf16[32,2176]{1,0:T(8,128)(2,1)S(1)}, bf16[32,2176]{1,0:T(8,128)(2,1)S(1)}, u32[]{:S(2)}, u32[]{:S(2)}) collective-permute-start(bf16[32,2176]{1,0:T(8,128)(2,1)S(1)} %get-tuple-element.35), channel_id=1, source_target_pairs={{0,24},{1,25},{2,26},{3,27},{4,28},{5,29},{6,30},{7,31},{8,0},{9,1... | collective-permute-start | bytes 417800 | tf_op jit(solution)/shard_map/ppermute | solution.py:150
  35.9 12.7 %collective-permute-start.11 = (bf16[32,2176]{1,0:T(8,128)(2,1)S(1)}, bf16[32,2176]{1,0:T(8,128)(2,1)S(1)}, u32[]{:S(2)}, u32[]{:S(2)}) collective-permute-start(bf16[32,2176]{1,0:T(8,128)(2,1)S(1)} %get-tuple-element.35), channel_id=1, source_target_pairs={{0,16},{1,17},{2,18},{3,19},{4,20},{5,21},{6,22},{7,23},{8,24},{9,... | collective-permute-start | bytes 417800 | tf_op jit(solution)/shard_map/ppermute | solution.py:150
  35.9 14.3 %collective-permute-start.1 = (bf16[32,2176]{1,0:T(8,128)(2,1)S(1)}, bf16[32,2176]{1,0:T(8,128)(2,1)S(1)}, u32[]{:S(2)}, u32[]{:S(2)}) collective-permute-start(bf16[32,2176]{1,0:T(8,128)(2,1)S(1)} %get-tuple-element.35), channel_id=1, source_target_pairs={{0,8},{1,9},{2,10},{3,11},{4,12},{5,13},{6,14},{7,15},{8,16},{9,17... | collective-permute-start | bytes 417800 | tf_op jit(solution)/shard_map/ppermute | solution.py:150
  48.6 6.6 %collective-permute-start.13 = (bf16[2,32,2176]{2,1,0:T(8,128)(2,1)S(1)}, bf16[2,32,2176]{2,1,0:T(8,128)(2,1)S(1)}, u32[]{:S(2)}, u32[]{:S(2)}) collective-permute-start(bf16[2,32,2176]{2,1,0:T(8,128)(2,1)S(1)} %get-tuple-element.29), channel_id=1, source_target_pairs={{0,2},{1,5},{2,0},{3,7},{4,6},{5,1},{6,4},{7,3},{8,10},{9,13},{10,... | collective-permute-start | bytes 835592 | tf_op jit(solution)/shard_map/ppermute | solution.py:150
  50.2 8.6 %collective-permute-start.2 = (bf16[2,32,2176]{2,1,0:T(8,128)(2,1)S(1)}, bf16[2,32,2176]{2,1,0:T(8,128)(2,1)S(1)}, u32[]{:S(2)}, u32[]{:S(2)}) collective-permute-start(bf16[2,32,2176]{2,1,0:T(8,128)(2,1)S(1)} %get-tuple-element.27), channel_id=1, source_target_pairs={{0,2},{1,5},{2,0},{3,7},{4,6},{5,1},{6,4},{7,3},{8,10},{9,13},{10,... | collective-permute-start | bytes 835592 | tf_op jit(solution)/shard_map/ppermute | solution.py:150
  56.1 9.8 %collective-permute-start.14 = (bf16[2,2,32,2176]{3,2,1,0:T(8,128)(2,1)}, bf16[2,2,32,2176]{3,2,1,0:T(8,128)(2,1)}, u32[]{:S(2)}, u32[]{:S(2)}) collective-permute-start(bf16[2,2,32,2176]{3,2,1,0:T(8,128)(2,1)} %pad_maximum_fusion.1), channel_id=1, source_target_pairs={{0,4},{1,3},{2,6},{3,1},{4,0},{5,7},{6,2},{7,5},{8,12},{9,11},{10,... | collective-permute-start | bytes 1671176 | tf_op jit(solution)/shard_map/ppermute | solution.py:150
  59.7 12.4 %collective-permute-start.3 = (bf16[2,2,32,2176]{3,2,1,0:T(8,128)(2,1)}, bf16[2,2,32,2176]{3,2,1,0:T(8,128)(2,1)}, u32[]{:S(2)}, u32[]{:S(2)}) collective-permute-start(bf16[2,2,32,2176]{3,2,1,0:T(8,128)(2,1)} %pad_maximum_fusion), channel_id=1, source_target_pairs={{0,4},{1,3},{2,6},{3,1},{4,0},{5,7},{6,2},{7,5},{8,12},{9,11},{10,... | collective-permute-start | bytes 1671176 | tf_op jit(solution)/shard_map/ppermute | solution.py:150
  61.2 11.0 %collective-permute-start.15 = (bf16[2,2,32,2176]{3,2,1,0:T(8,128)(2,1)}, bf16[2,2,32,2176]{3,2,1,0:T(8,128)(2,1)}, u32[]{:S(2)}, u32[]{:S(2)}) collective-permute-start(bf16[2,2,32,2176]{3,2,1,0:T(8,128)(2,1)} %pad_maximum_fusion.1), channel_id=1, source_target_pairs={{0,1},{1,0},{2,3},{3,2},{4,5},{5,4},{6,7},{7,6},{8,9},{9,8},{10,11... | collective-permute-start | bytes 1671176 | tf_op jit(solution)/shard_map/ppermute | solution.py:154
  65.9 6.2 %collective-permute-start.16 = (bf16[2,2,32,2176]{3,2,1,0:T(8,128)(2,1)}, bf16[2,2,32,2176]{3,2,1,0:T(8,128)(2,1)}, u32[]{:S(2)}, u32[]{:S(2)}) collective-permute-start(bf16[2,2,32,2176]{3,2,1,0:T(8,128)(2,1)} %collective-permute-done.14), channel_id=1, source_target_pairs={{0,1},{1,0},{2,3},{3,2},{4,5},{5,4},{6,7},{7,6},{8,9},{9,8},{10,11... | collective-permute-start | bytes 1671176 | tf_op jit(solution)/shard_map/ppermute | solution.py:154
  67.9 2.5 %copy-start.6 = (bf16[176,2048]{1,0:T(8,128)(2,1)S(1)}, bf16[176,2048]{1,0:T(8,128)(2,1)}, u32[]{:S(2)}) copy-start(bf16[176,2048]{1,0:T(8,128)(2,1)} %dense_down_ref.3) | copy-start | bytes 2162692
  68.4 3.8 %copy-start.3 = (bf16[1,2048,768]{2,1,0:T(8,128)(2,1)S(1)}, bf16[1,2048,768]{2,1,0:T(8,128)(2,1)}, u32[]{:S(2)}) copy-start(bf16[1,2048,768]{2,1,0:T(8,128)(2,1)} %expert_up_ref.3) | copy-start | bytes 9437188
  71.5 8.3 %collective-permute-start.4 = (bf16[2,2,32,2176]{3,2,1,0:T(8,128)(2,1)}, bf16[2,2,32,2176]{3,2,1,0:T(8,128)(2,1)S(1)}, u32[]{:S(2)}, u32[]{:S(2)}) collective-permute-start(bf16[2,2,32,2176]{3,2,1,0:T(8,128)(2,1)} %pad_maximum_fusion), channel_id=1, source_target_pairs={{0,1},{1,0},{2,3},{3,2},{4,5},{5,4},{6,7},{7,6},{8,9},{9,8},{10,11... | collective-permute-start | bytes 1671176 | tf_op jit(solution)/shard_map/ppermute | solution.py:154
  72.1 7.8 %collective-permute-start.5 = (bf16[2,2,32,2176]{3,2,1,0:T(8,128)(2,1)}, bf16[2,2,32,2176]{3,2,1,0:T(8,128)(2,1)S(1)}, u32[]{:S(2)}, u32[]{:S(2)}) collective-permute-start(bf16[2,2,32,2176]{3,2,1,0:T(8,128)(2,1)} %collective-permute-done.3), channel_id=1, source_target_pairs={{0,1},{1,0},{2,3},{3,2},{4,5},{5,4},{6,7},{7,6},{8,9},{9,8},{10,11... | collective-permute-start | bytes 1671176 | tf_op jit(solution)/shard_map/ppermute | solution.py:154
  79.4 7.9 %collective-permute-start.18 = (bf16[2,2,32,2048]{3,2,1,0:T(8,128)(2,1)S(1)}, bf16[2,2,32,2048]{3,2,1,0:T(8,128)(2,1)S(1)}, u32[]{:S(2)}, u32[]{:S(2)}) collective-permute-start(bf16[2,2,32,2048]{3,2,1,0:T(8,128)(2,1)S(1)} %bitcast.87), channel_id=1, source_target_pairs={{0,1},{1,0},{2,3},{3,2},{4,5},{5,4},{6,7},{7,6},{8,9},{9,8},{10,11... | collective-permute-start | bytes 1572872 | tf_op jit(solution)/shard_map/ppermute | solution.py:154
  86.7 2.3 %collective-permute-start.7 = (bf16[2,2,32,2048]{3,2,1,0:T(8,128)(2,1)S(1)}, bf16[2,2,32,2048]{3,2,1,0:T(8,128)(2,1)S(1)}, u32[]{:S(2)}, u32[]{:S(2)}) collective-permute-start(bf16[2,2,32,2048]{3,2,1,0:T(8,128)(2,1)S(1)} %bitcast.88), channel_id=1, source_target_pairs={{0,1},{1,0},{2,3},{3,2},{4,5},{5,4},{6,7},{7,6},{8,9},{9,8},{10,11... | collective-permute-start | bytes 1572872 | tf_op jit(solution)/shard_map/ppermute | solution.py:154
  86.9 3.7 %collective-permute-start.17 = (bf16[2,2,32,2048]{3,2,1,0:T(8,128)(2,1)S(1)}, bf16[2,2,32,2048]{3,2,1,0:T(8,128)(2,1)S(1)}, u32[]{:S(2)}, u32[]{:S(2)}) collective-permute-start(bf16[2,2,32,2048]{3,2,1,0:T(8,128)(2,1)S(1)} %bitcast.85), channel_id=1, source_target_pairs={{0,1},{1,0},{2,3},{3,2},{4,5},{5,4},{6,7},{7,6},{8,9},{9,8},{10,11... | collective-permute-start | bytes 1572872 | tf_op jit(solution)/shard_map/ppermute | solution.py:154
  87.4 9.2 %collective-permute-start.19 = (bf16[2,2,32,2048]{3,2,1,0:T(8,128)(2,1)S(1)}, bf16[2,2,32,2048]{3,2,1,0:T(8,128)(2,1)S(1)}, u32[]{:S(2)}, u32[]{:S(2)}) collective-permute-start(bf16[2,2,32,2048]{3,2,1,0:T(8,128)(2,1)S(1)} %fusion), channel_id=1, source_target_pairs={{0,4},{1,3},{2,6},{3,1},{4,0},{5,7},{6,2},{7,5},{8,12},{9,11},{10,... | collective-permute-start | bytes 1572872 | tf_op jit(solution)/shard_map/ppermute | solution.py:150
  89.0 9.5 %collective-permute-start.6 = (bf16[2,2,32,2048]{3,2,1,0:T(8,128)(2,1)S(1)}, bf16[2,2,32,2048]{3,2,1,0:T(8,128)(2,1)S(1)}, u32[]{:S(2)}, u32[]{:S(2)}) collective-permute-start(bf16[2,2,32,2048]{3,2,1,0:T(8,128)(2,1)S(1)} %bitcast.86), channel_id=1, source_target_pairs={{0,1},{1,0},{2,3},{3,2},{4,5},{5,4},{6,7},{7,6},{8,9},{9,8},{10,11... | collective-permute-start | bytes 1572872 | tf_op jit(solution)/shard_map/ppermute | solution.py:154
  89.1 15.9 %collective-permute-start.8 = (bf16[2,2,32,2048]{3,2,1,0:T(8,128)(2,1)S(1)}, bf16[2,2,32,2048]{3,2,1,0:T(8,128)(2,1)S(1)}, u32[]{:S(2)}, u32[]{:S(2)}) collective-permute-start(bf16[2,2,32,2048]{3,2,1,0:T(8,128)(2,1)S(1)} %fusion.3), channel_id=1, source_target_pairs={{0,4},{1,3},{2,6},{3,1},{4,0},{5,7},{6,2},{7,5},{8,12},{9,11},{10,... | collective-permute-start | bytes 1572872 | tf_op jit(solution)/shard_map/ppermute | solution.py:150
  96.9 10.0 %collective-permute-start.20 = (bf16[2,32,2048]{2,1,0:T(8,128)(2,1)S(1)}, bf16[2,32,2048]{2,1,0:T(8,128)(2,1)S(1)}, u32[]{:S(2)}, u32[]{:S(2)}) collective-permute-start(bf16[2,32,2048]{2,1,0:T(8,128)(2,1)S(1)} %slice_bitcast_fusion), channel_id=1, source_target_pairs={{0,2},{1,5},{2,0},{3,7},{4,6},{5,1},{6,4},{7,3},{8,10},{9,13},{10,... | collective-permute-start | bytes 786440 | tf_op jit(solution)/shard_map/ppermute | solution.py:150
  105.4 6.4 %collective-permute-start.9 = (bf16[2,32,2048]{2,1,0:T(8,128)(2,1)S(1)}, bf16[2,32,2048]{2,1,0:T(8,128)(2,1)S(1)}, u32[]{:S(2)}, u32[]{:S(2)}) collective-permute-start(bf16[2,32,2048]{2,1,0:T(8,128)(2,1)S(1)} %slice_bitcast_fusion.2), channel_id=1, source_target_pairs={{0,2},{1,5},{2,0},{3,7},{4,6},{5,1},{6,4},{7,3},{8,10},{9,13},{10,... | collective-permute-start | bytes 786440 | tf_op jit(solution)/shard_map/ppermute | solution.py:150
  107.0 7.7 %collective-permute-start.22 = (bf16[32,2048]{1,0:T(8,128)(2,1)S(1)}, bf16[32,2048]{1,0:T(8,128)(2,1)S(1)}, u32[]{:S(2)}, u32[]{:S(2)}) collective-permute-start(bf16[32,2048]{1,0:T(8,128)(2,1)S(1)} %get-tuple-element.33), channel_id=1, source_target_pairs={{0,8},{1,9},{2,10},{3,11},{4,12},{5,13},{6,14},{7,15},{8,16},{9,17... | collective-permute-start | bytes 393224 | tf_op jit(solution)/shard_map/ppermute | solution.py:150
  107.1 10.5 %collective-permute-start.21 = (bf16[32,2048]{1,0:T(8,128)(2,1)S(1)}, bf16[32,2048]{1,0:T(8,128)(2,1)S(1)}, u32[]{:S(2)}, u32[]{:S(2)}) collective-permute-start(bf16[32,2048]{1,0:T(8,128)(2,1)S(1)} %get-tuple-element.32), channel_id=1, source_target_pairs={{0,16},{1,17},{2,18},{3,19},{4,20},{5,21},{6,22},{7,23},{8,24},{9,... | collective-permute-start | bytes 393224 | tf_op jit(solution)/shard_map/ppermute | solution.py:150
  111.9 5.8 %collective-permute-start.10 = (bf16[32,2048]{1,0:T(8,128)(2,1)S(1)}, bf16[32,2048]{1,0:T(8,128)(2,1)S(1)}, u32[]{:S(2)}, u32[]{:S(2)}) collective-permute-start(bf16[32,2048]{1,0:T(8,128)(2,1)S(1)} %slice_bitcast_fusion.6), channel_id=1, source_target_pairs={{0,24},{1,25},{2,26},{3,27},{4,28},{5,29},{6,30},{7,31},{8,0},{9,1... | collective-permute-start | bytes 393224 | tf_op jit(solution)/shard_map/ppermute | solution.py:150
  117.7 1.4 %collective-permute-start.23 = (bf16[32,2048]{1,0:T(8,128)(2,1)S(1)}, bf16[32,2048]{1,0:T(8,128)(2,1)S(1)}, u32[]{:S(2)}, u32[]{:S(2)}) collective-permute-start(bf16[32,2048]{1,0:T(8,128)(2,1)S(1)} %fusion.14), channel_id=1, source_target_pairs={{0,1},{1,0},{2,3},{3,2},{4,5},{5,4},{6,7},{7,6},{8,9},{9,8},{10,11... | collective-permute-start | bytes 393224 | tf_op jit(solution)/shard_map/ppermute | solution.py:154
  (4 other events, 8.1 us)
